TPU v7x, 32 devices: a whole 2x2x4 slice. The times are simulated.
32 devices in a mesh: ep: 8 (over z, x), tp: 4 (over y, core).
Axes of the slice: x: 2, y: 2, z: 4, core: 2. Of those that a mesh axis runs over, the one named last changes fastest.
Arguments:
- mix_rows: bfloat16 [2048, 2048], P('ep'), may hold values from -6 to 6
- mix_gain: bfloat16 [2048], replicated, may hold values from 0.099609375 to 1.8984375
- w_query: bfloat16 [1024, 2048], P('tp'), may hold values from -0.125 to 0.125
- w_key: bfloat16 [1024, 2048], P('tp'), may hold values from -0.125 to 0.125
- w_value: bfloat16 [1024, 2048], P('tp'), may hold values from -0.125 to 0.125
- key_offset: float32 [16, 2048], P('tp'), may hold values from -11 to 0
- w_out: bfloat16 [1024, 2048], P('tp'), may hold values from -0.1875 to 0.1875
- out_gain: bfloat16 [2048], replicated, may hold values from 0.099609375 to 1.8984375
- exp_rows: bfloat16 [768, 2048], P('ep', 'tp'), may hold values from -100 to 100
- exp_gain: bfloat16 [2048], P('tp'), may hold values from 0.099609375 to 1.8984375
- routes: int32 [768, 4], P('ep'), may hold values from 0 to 7, all different within a row; in each aligned block of 96 rows (0 to 95, 96 to 191, ...) at most 64 rows name the same one
- route_weight: float32 [768, 4], P('ep'), may hold values from 0.05 to 1
- w_gate: bfloat16 [8, 2048, 2048], P('ep', None, 'tp'), may hold values from -0.5 to 0.5
- w_up: bfloat16 [8, 2048, 2048], P('ep', None, 'tp'), may hold values from -0.5 to 0.5
- w_down: bfloat16 [8, 2048, 2048], P('ep', 'tp'), may hold values from -0.1875 to 0.1875
Outputs:
- mix_out: bfloat16 [2048, 2048], P('ep')
- exp_out: bfloat16 [768, 2048], P('ep', 'tp')
Inputs may be any that keep to these rules, and one draw needn't show every extreme that they name: `routes`: each row names 4 different experts. Within the rows of one device (aligned blocks of 96 rows) no expert is named by more than 64 rows, and in some blocks one expert is named by exactly 64 rows.
All inputs are finite; a program needn't handle non-finite values.
Results may differ from a plain program's by a relative error of at most 0.019.
Values may be sent and summed in bfloat16 or wider, within the bound.
A program may use at most 128 MiB of HBM per device.

v0:
```python
import functools
import math

import jax
import jax.numpy as jnp
from jax import lax
from jax.experimental import pallas as pl
from jax.experimental.pallas import tpu as pltpu
from jax.sharding import PartitionSpec as P

EPSILON = 1e-06
CLAMP_LIMIT = 7.0
SILU_SHARPNESS = 1.702
MESH = pl.DeviceIdType.MESH


def normalize(numbers, gain):
    factor = lax.rsqrt(jnp.mean(numbers * numbers, axis=-1, keepdims=True) + EPSILON)
    return numbers * factor * gain.astype(jnp.float32)


def project(normed, weight):
    product = lax.dot_general(
        normed, weight, (((1,), (1,)), ((), ())), preferred_element_type=jnp.float32
    )
    return product.astype(jnp.bfloat16)


def gated_units(gate_pre, up_pre):
    gate_part = jnp.minimum(gate_pre, CLAMP_LIMIT)
    up_part = jnp.clip(up_pre, -CLAMP_LIMIT, CLAMP_LIMIT)
    return (up_part + 1.0) * (gate_part * jax.nn.sigmoid(SILU_SHARPNESS * gate_part))


def stick_block(q, kv, off, carry, acc, later, visible):
    scores = (
        lax.dot_general(q, kv, (((1,), (1,)), ((), ())), preferred_element_type=jnp.float32) + off
    )
    keep = -(jnp.maximum(scores, 0.0) + jnp.log(1.0 + jnp.exp(-jnp.abs(scores))))
    own = scores + keep
    if visible is not None:
        keep = jnp.where(visible, keep, 0.0)
    beyond = jnp.dot(keep.astype(jnp.bfloat16), later, preferred_element_type=jnp.float32)
    weights = jnp.exp(own + beyond + carry)
    if visible is not None:
        weights = jnp.where(visible, weights, 0.0)
    acc = acc + jnp.dot(weights.astype(jnp.bfloat16), kv, preferred_element_type=jnp.float32)
    return carry + jnp.sum(keep, axis=1, keepdims=True), acc


def kernel(
    dims, kv_ref, q_ref, off_ref, exp_ref, gain_ref, wg_hbm, wu_hbm, wd_hbm, wo_hbm, mix_gain,
    out_ref, ret_ref,
    kv_all, q_all, seg_ref, wg_ref, wu_ref, wd_ref, wo_ref, sum_ref, e_got, e_pair, e_y, e_fin,
    att_ref, att_all, att_rows, m_send, m_got, m_sum,
    kv_send, kv_recv, q_send, q_recv, x_send, x_recv, p_send, p_recv, g_send, g_recv,
    f_send, f_recv, d_send, d_recv, y_send, y_recv, z_send, z_recv, a_send, a_recv,
    h_send, h_recv, v_send, v_recv, o_send, o_recv, own_sem, w_sem,
):
    ep, tp, share, part, packed = dims
    chips = tp // 2
    heads = ep // share
    me = lax.axis_index("ep")
    mt = lax.axis_index("tp")
    core = lax.rem(mt, 2)
    partner = mt + 1 - 2 * core
    cap, width = exp_ref.shape[1:]
    block = kv_ref.shape[1]
    half = out_ref.shape[0] // 2
    pieces = o_send.shape[0]
    piece = half // pieces
    groups = d_send.shape[1]
    per = ep // groups

    def peer(s):
        return lax.rem(me + s, ep)

    def before(s):
        return lax.rem(me - s + ep, ep)

    def other(k):
        return lax.rem(mt + 2 * k, tp)

    weights = [
        pltpu.make_async_copy(src, dst, w_sem.at[i])
        for i, (src, dst) in enumerate(
            [(wg_hbm, wg_ref), (wu_hbm, wu_ref), (wd_hbm, wd_ref), (wo_hbm, wo_ref)]
        )
    ]
    for copy in weights:
        copy.start()

    barrier = pltpu.get_barrier_semaphore()

    def greet(s, _):
        pl.semaphore_signal(barrier, inc=1, device_id={"ep": peer(s)}, device_id_type=MESH)
        return 0

    lax.fori_loop(1, ep, greet, 0)
    pl.semaphore_signal(barrier, inc=1, device_id={"tp": partner}, device_id_type=MESH)
    for k in range(1, chips):
        pl.semaphore_signal(barrier, inc=1, device_id={"tp": other(k)}, device_id_type=MESH)
    pl.semaphore_wait(barrier, ep - 1 + 1 + chips - 1)

    def remote(src, dst, send, recv, where):
        return pltpu.make_async_remote_copy(
            src_ref=src, dst_ref=dst, send_sem=send, recv_sem=recv,
            device_id=where, device_id_type=MESH,
        )

    def rows(s):
        return pl.ds(s * cap, cap)

    def columns(t):
        return pl.ds(pl.multiple_of(t * width, 128), width)

    def x_copy(s):
        return remote(
            exp_ref.at[peer(s)], seg_ref.at[rows(s), columns(mt)], x_send.at[s], x_recv.at[s],
            {"ep": peer(s)},
        )

    def kv_copy(dest, slot):
        return remote(
            kv_ref.at[dest // share], kv_all.at[slot], kv_send.at[dest], kv_recv.at[slot],
            {"ep": dest},
        )

    def q_copy(dest, slot):
        return remote(
            q_ref.at[dest], q_all.at[slot], q_send.at[dest], q_recv.at[slot], {"ep": dest}
        )

    tail = pl.ds(ep * cap, gain_ref.shape[0])
    own_x = pltpu.make_async_copy(exp_ref.at[me], seg_ref.at[rows(0), columns(mt)], own_sem.at[2])
    own_g = pltpu.make_async_copy(gain_ref, seg_ref.at[tail, columns(mt)], own_sem.at[3])
    own_kv = pltpu.make_async_copy(kv_ref.at[me // share], kv_all.at[me], own_sem.at[0])
    own_q = pltpu.make_async_copy(q_ref.at[me], q_all.at[me], own_sem.at[1])
    for copy in (own_x, own_g, own_kv, own_q):
        copy.start()
    for s in range(1, ep):
        x_copy(s).start()

    def send_mix(s, _):
        q_copy(peer(s), me).start()
        kv_copy(peer(s), me).start()
        return 0

    lax.fori_loop(1, ep, send_mix, 0)
    for copy in (own_x, own_g, own_kv, own_q):
        copy.wait()

    def rows_of(n):
        return tail if n == ep else rows(n)

    def p_copy(n):
        at = seg_ref.at[rows_of(n), columns(mt)]
        return remote(at, at, p_send.at[n], p_recv.at[n], {"tp": partner})

    def g_copy(n, k):
        at = seg_ref.at[rows_of(n), columns(mt)]
        return remote(at, at, g_send.at[k, n], g_recv.at[k, n], {"tp": other(k)})

    def f_copy(n, k):
        at = seg_ref.at[rows_of(n), columns(lax.rem(mt - 2 * k + tp, tp))]
        return remote(at, at, f_send.at[k, n], f_recv.at[k, n], {"tp": partner})

    def spread(n):
        if 0 < n < ep:
            x_copy(n).wait_recv()
        for k in range(1, chips):
            g_copy(n, k).start()
        p_copy(n).start()

    def forward(n):
        for k in range(1, chips):
            g_copy(n, k).wait_recv()
            f_copy(n, k).start()

    def gathered(n):
        p_copy(n).wait_recv()
        for k in range(1, chips):
            f_copy(n, k).wait_recv()

    def d_copy(k, g):
        at = pl.ds(g * per * cap, per * cap)
        return remote(
            sum_ref.at[at, columns(lax.rem(partner + 2 * k, tp))], e_got.at[k, at],
            d_send.at[k, g], d_recv.at[k, g], {"tp": partner},
        )

    def y_copy(k, s):
        return remote(
            e_pair.at[k - 1, rows(s)], e_y.at[k - 1, rows(s)], y_send.at[k, s],
            y_recv.at[k, s], {"tp": other(k)},
        )

    def z_copy(s):
        place = ret_ref.at[pl.ds(pl.multiple_of(me * cap, cap), cap)]
        return remote(
            e_fin.at[rows(s)], place, z_send.at[s], z_recv.at[s], {"ep": before(s)}
        )

    def z_arrived(s):
        place = ret_ref.at[pl.ds(pl.multiple_of(peer(s) * cap, cap), cap)]
        return remote(
            e_fin.at[rows(s)], place, z_send.at[s], z_recv.at[s], {"ep": before(s)}
        )

    def expert(g):
        at = pl.ds(g * per * cap, per * cap)
        gains = seg_ref[tail, :][:1]
        segment = normalize(seg_ref[at, :].astype(jnp.float32), gains).astype(jnp.bfloat16)
        gate_pre = jnp.dot(segment, wg_ref[...], preferred_element_type=jnp.float32)
        up_pre = jnp.dot(segment, wu_ref[...], preferred_element_type=jnp.float32)
        hidden = gated_units(gate_pre, up_pre).astype(jnp.bfloat16)
        sum_ref[at, :] = jnp.dot(
            hidden, wd_ref[...], preferred_element_type=jnp.float32
        ).astype(jnp.bfloat16)
        for k in list(range(1, chips)) + [0]:
            d_copy(k, g).start()

    def pair(g):
        for k in range(1, chips):
            d_copy(k, g).wait_recv()
        for s in range(g * per, (g + 1) * per):
            for k in range(1, chips):
                mine = sum_ref[rows(s), columns(other(k))].astype(jnp.float32)
                both = mine + e_got[k, rows(s), :].astype(jnp.float32)
                e_pair[k - 1, rows(s), :] = both.astype(jnp.bfloat16)
                y_copy(k, s).start()
        d_copy(0, g).wait_recv()

    own_fin = pltpu.make_async_copy(
        e_fin.at[rows(0)], ret_ref.at[pl.ds(pl.multiple_of(me * cap, cap), cap)], own_sem.at[4]
    )

    def fin(s):
        total = sum_ref[rows(s), columns(mt)].astype(jnp.float32)
        total = total + e_got[0, rows(s), :].astype(jnp.float32)
        for k in range(1, chips):
            y_copy(k, s).wait_recv()
            total = total + e_y[k - 1, rows(s), :].astype(jnp.float32)
        e_fin[rows(s), :] = total.astype(jnp.bfloat16)
        if s > 0:
            z_copy(s).start()
        else:
            own_fin.start()

    spread(ep)
    for g in range(groups):
        lag = 2
        first, last = g * per, (g + 1) * per
        for s in range(first, last):
            spread(s)
            if s == 1:
                forward(ep)
            if s - lag >= first:
                forward(s - lag)
        if ep == 1:
            forward(ep)
        for s in range(max(first, last - lag), last):
            forward(s)
        if g == 0:
            gathered(ep)
            for copy in weights:
                copy.wait()
        else:
            pair(g - 1)
        for s in range(first, last):
            gathered(s)
        expert(g)

    def q_wait(s, _):
        q_copy(peer(s), before(s)).wait_recv()
        return 0

    lax.fori_loop(1, ep, q_wait, 0)
    lane = lax.broadcasted_iota(jnp.int32, (1, 128), 1)

    def queries(i):
        both = q_all[i].astype(jnp.float32)
        if packed:
            both = jnp.concatenate([both, pltpu.roll(both, 64, 1)], axis=0)
        return jnp.where(lane < 64, both, 0.0).astype(jnp.bfloat16)

    later = (
        lax.broadcasted_iota(jnp.int32, (block, block), 0)
        > lax.broadcasted_iota(jnp.int32, (block, block), 1)
    ).astype(jnp.float32).astype(jnp.bfloat16)
    row = lax.broadcasted_iota(jnp.int32, (part, block), 0) + lax.rem(me, share) * part
    visible = lax.broadcasted_iota(jnp.int32, (part, block), 1) < row
    carry = acc = q_rest = None
    done = 0
    for n in range(ep):
        j = ep - 1 - n

        @pl.when(me != j)
        def _():
            kv_copy(lax.rem(2 * me - j + ep, ep), j).wait_recv()

        kv = kv_all[j]
        off = off_ref[j]
        q = queries(j)
        zero_carry = jnp.zeros((part, 1), jnp.float32)
        zero_acc = jnp.zeros((part, 128), jnp.float32)
        new_carry, new_acc = stick_block(q, kv, off, zero_carry, zero_acc, later, visible)
        if n == 0:
            carry, acc, q_rest = new_carry, new_acc, q
        else:
            carry, acc = stick_block(q_rest, kv, off, carry, acc, later, None)
            carry = jnp.concatenate([new_carry, carry], axis=0)
            acc = jnp.concatenate([new_acc, acc], axis=0)
            q_rest = jnp.concatenate([q, q_rest], axis=0)
        if n == min(1, ep - 1):
            pair(groups - 1)
        if n >= 1:
            fin(done)
            done = done + 1
    for i in range(ep):
        block_out = acc[i * part : (i + 1) * part]
        if packed:
            middle = part // 2
            block_out = jnp.where(
                lane < 64, pltpu.roll(block_out[:middle], 64, 1), block_out[middle:]
            )
        att_ref[i] = block_out.astype(jnp.bfloat16)

    def a_copy(dest, slot):
        return remote(
            att_ref.at[dest], att_all.at[slot], a_send.at[dest], a_recv.at[slot], {"ep": dest}
        )

    def start_a(s, _):
        a_copy(peer(s), me).start()
        return 0

    lax.fori_loop(1, ep, start_a, 0)
    own_att = pltpu.make_async_copy(att_ref.at[me], att_all.at[me], own_sem.at[5])
    own_att.start()
    for s in range(done, ep):
        fin(s)
    own_att.wait()

    def wait_a(s, _):
        a_copy(peer(s), before(s)).wait_recv()
        return 0

    lax.fori_loop(1, ep, wait_a, 0)
    for r in range(share):
        got = [att_all[h * share + r].astype(jnp.float32) for h in range(heads)]
        if packed and heads % 2 == 0:
            upper = []
            lower = []
            for h in range(0, heads, 2):
                upper.append(jnp.where(lane < 64, got[h], pltpu.roll(got[h + 1], 64, 1)))
                lower.append(jnp.where(lane < 64, pltpu.roll(got[h], 64, 1), got[h + 1]))
            both = jnp.concatenate(
                [jnp.concatenate(upper, axis=1), jnp.concatenate(lower, axis=1)], axis=0
            )
        else:
            both = []
            for h in range(heads):
                whole = got[h]
                if packed:
                    whole = jnp.concatenate([pltpu.roll(whole, 64, 1), whole], axis=0)
                both.append(jnp.where(lane < 64, 0.0, whole))
            both = jnp.concatenate(both, axis=1)
        att_rows[pl.ds(r * part, part), :] = both.astype(jnp.bfloat16)

    def half_rows(c):
        return pl.ds(pl.multiple_of(c * half, half), half)

    h_copy = remote(m_send, m_got, h_send.at[0], h_recv.at[0], {"tp": partner})
    m_send[...] = jnp.dot(
        att_rows[half_rows(1 - core), :], wo_ref[...], preferred_element_type=jnp.float32
    ).astype(jnp.bfloat16)
    h_copy.start()
    mine = jnp.dot(att_rows[half_rows(core), :], wo_ref[...], preferred_element_type=jnp.float32)
    h_copy.wait_recv()

    def v_copy(k, i):
        at = pl.ds(i * piece, piece)
        return remote(
            m_sum.at[0, at], m_sum.at[k, at], v_send.at[k, i], v_recv.at[k, i],
            {"tp": other(k)},
        )

    for i in range(pieces):
        at = pl.ds(i * piece, piece)
        pair = mine[i * piece : (i + 1) * piece] + m_got[at, :].astype(jnp.float32)
        m_sum[0, at, :] = pair.astype(jnp.bfloat16)
        for k in range(1, chips):
            v_copy(k, i).start()

    def o_copy(i):
        at = out_ref.at[pl.ds(pl.multiple_of(core * half + i * piece, piece), piece)]
        return remote(at, at, o_send.at[i], o_recv.at[i], {"tp": partner})

    gain = mix_gain[...].astype(jnp.float32)
    for i in range(pieces):
        at = pl.ds(i * piece, piece)
        for k in range(1, chips):
            v_copy(k, i).wait_recv()
        total = jnp.zeros((piece, out_ref.shape[1]), jnp.float32)
        for chip in range(chips):
            slot = lax.rem(mt // 2 - chip + chips, chips)
            total = total + m_sum[slot, at, :].astype(jnp.float32)
        own_rows = pl.ds(pl.multiple_of(core * half + i * piece, piece), piece)
        out_ref[own_rows, :] = normalize(total, gain).astype(jnp.bfloat16)
        o_copy(i).start()

    own_fin.wait()
    h_copy.wait_send()
    for n in range(ep + 1):
        p_copy(n).wait_send()
        for k in range(1, chips):
            g_copy(n, k).wait_send()
            f_copy(n, k).wait_send()
    for k in range(chips):
        for g in range(groups):
            d_copy(k, g).wait_send()
    for k in range(1, chips):
        for s in range(ep):
            y_copy(k, s).wait_send()
        for i in range(pieces):
            v_copy(k, i).wait_send()
    for s in range(1, ep):
        x_copy(s).wait_send()
        z_copy(s).wait_send()
        z_arrived(s).wait_recv()

    def finish(s, _):
        q_copy(peer(s), me).wait_send()
        kv_copy(peer(s), me).wait_send()
        a_copy(peer(s), me).wait_send()
        return 0

    lax.fori_loop(1, ep, finish, 0)
    for i in range(pieces):
        at = out_ref.at[pl.ds(pl.multiple_of((1 - core) * half + i * piece, piece), piece)]
        remote(at, at, o_send.at[i], o_recv.at[i], {"tp": partner}).wait_recv()
        o_copy(i).wait_send()


def one_call(ep, tp, share, part, packed, kv, q, off, outgoing, gain, wg, wu, wd, wo, out_gain):
    cap, width = outgoing.shape[1:]
    slots, full = ep * cap, tp * width
    chips = tp // 2
    row_count = share * part
    half = row_count // 2
    pieces = 4
    groups = 2 if ep % 2 == 0 else 1
    others = max(chips - 1, 1)
    dma = pltpu.SemaphoreType.DMA
    vmem = pl.BlockSpec(memory_space=pltpu.VMEM)
    hbm = pl.BlockSpec(memory_space=pl.ANY)

    def held(*shape):
        return pltpu.VMEM(shape, jnp.bfloat16)

    def both(*shape):
        return [dma(shape), dma(shape)]

    return pl.pallas_call(
        functools.partial(kernel, (ep, tp, share, part, packed)),
        out_shape=(
            jax.ShapeDtypeStruct((row_count, full), jnp.bfloat16),
            jax.ShapeDtypeStruct((slots, width), jnp.bfloat16),
        ),
        in_specs=[vmem] * 5 + [hbm] * 4 + [vmem],
        out_specs=(vmem, vmem),
        scratch_shapes=[
            held(ep, *kv.shape[1:]), held(ep, *q.shape[1:]),
            held(slots + gain.shape[0], full),
            held(*wg.shape), held(*wu.shape), held(*wd.shape), held(*wo.shape),
            held(slots, full), held(chips, slots, width), held(others, slots, width),
            held(others, slots, width), held(slots, width),
            held(*q.shape), held(*q.shape), held(row_count, wo.shape[0]),
            held(half, full), held(half, full), held(chips, half, full),
        ]
        + both(ep) + both(ep) + both(ep) + both(ep + 1) + both(chips, ep + 1)
        + both(chips, ep + 1) + both(chips, groups) + both(chips, ep) + both(ep) + both(ep)
        + both(1) + both(chips, pieces) + both(pieces) + [dma((6,)), dma((4,))],
        compiler_params=pltpu.CompilerParams(
            collective_id=0, has_side_effects=True, vmem_limit_bytes=60 * 1024 * 1024
        ),
    )(kv, q, off, outgoing, gain, wg, wu, wd, wo, out_gain)


def on_device(
    mix_rows,
    mix_gain,
    w_query,
    w_key,
    w_value,
    key_offset,
    w_out,
    out_gain,
    exp_rows,
    exp_gain,
    routes,
    route_weight,
    w_gate,
    w_up,
    w_down,
):
    ep = lax.axis_size("ep")
    tp = lax.axis_size("tp")
    row_count = mix_rows.shape[0]
    heads_here = key_offset.shape[0]
    head_size = w_query.shape[0] // heads_here
    share = ep // heads_here
    part = row_count // share
    packed = part % 32 == 0
    normed = normalize(mix_rows.astype(jnp.float32), mix_gain).astype(jnp.bfloat16)
    queries = project(normed, w_query) * jnp.bfloat16(1.0 / math.sqrt(head_size))
    keys = project(normed, w_key).reshape(row_count, heads_here, 1, head_size)
    values = project(normed, w_value).reshape(row_count, heads_here, 1, head_size)
    kv = jnp.concatenate([keys, values], axis=2).reshape(row_count, heads_here, 2 * head_size)
    kv = kv.transpose(1, 0, 2)
    q = queries.reshape(share, part, heads_here, head_size).transpose(2, 0, 1, 3)
    q = q.reshape(ep, part, head_size)
    if packed:
        q = jnp.concatenate([q[:, : part // 2], q[:, part // 2 :]], axis=2)
    else:
        q = jnp.concatenate([q, jnp.zeros_like(q)], axis=2)
    off = lax.dynamic_slice_in_dim(key_offset, lax.axis_index("ep") // share, 1, 0)
    off = off.reshape(ep, 1, row_count)

    token_count, top_count = routes.shape
    experts = w_gate.shape[0] * ep
    capacity = 4 * token_count * top_count // (3 * experts)
    named = routes[:, :, None] == jnp.arange(experts, dtype=jnp.int32)
    chosen = jnp.any(named, axis=1)
    weight = jnp.sum(jnp.where(named, route_weight[:, :, None], 0.0), axis=1)
    before = jnp.tril(jnp.ones((token_count, token_count), jnp.bfloat16), -1)
    slot = jnp.dot(before, chosen.astype(jnp.bfloat16), preferred_element_type=jnp.float32)
    placed = chosen[:, :, None] & (
        slot.astype(jnp.int32)[:, :, None] == jnp.arange(capacity, dtype=jnp.int32)
    )
    flat = placed.reshape(token_count, experts * capacity)
    outgoing = lax.dot_general(
        flat.astype(jnp.bfloat16), exp_rows, (((0,), (0,)), ((), ())),
        preferred_element_type=jnp.float32,
    ).astype(jnp.bfloat16)
    outgoing = outgoing.reshape(experts, capacity, -1)
    gain = jnp.broadcast_to(exp_gain[None], (16, exp_gain.shape[0]))

    slots = experts * capacity
    if not (packed and heads_here % 2 == 0):
        w_out = w_out.reshape(heads_here, head_size, -1)
        w_out = jnp.concatenate([jnp.zeros_like(w_out), w_out], axis=1)
        w_out = w_out.reshape(2 * heads_here * head_size, -1)
    mix_out, returned = one_call(
        ep, tp, share, part, packed, kv, q, off, outgoing, gain,
        w_gate[0], w_up[0], w_down[0], w_out, out_gain[None],
    )
    spread = jnp.where(placed, weight[:, :, None], 0.0).reshape(token_count, slots)
    high = spread.astype(jnp.bfloat16)
    low = (spread - high.astype(jnp.float32)).astype(jnp.bfloat16)
    exp_out = sum(
        lax.dot_general(
            part_of, returned, (((1,), (0,)), ((), ())), preferred_element_type=jnp.float32
        )
        for part_of in (high, low)
    ).astype(jnp.bfloat16)
    return (mix_out, exp_out)


def solution(mesh):
    placed = (
        P("ep", None),
        P(),
        P("tp", None),
        P("tp", None),
        P("tp", None),
        P("tp", None),
        P("tp", None),
        P(),
        P("ep", "tp"),
        P("tp"),
        P("ep", None),
        P("ep", None),
        P("ep", None, "tp"),
        P("ep", None, "tp"),
        P("ep", "tp", None),
    )
    return jax.shard_map(
        on_device,
        mesh=mesh,
        in_specs=placed,
        out_specs=(P("ep", None), P("ep", "tp")),
        check_vma=False,
    )
```

profile of v0, /device:TPU:0, one launch (start us, length us, event | category | flops | bytes accessed | tf_op | source)
XLA Modules:
  0.0 91.4 jit_solution(14410212175882866650)
XLA Ops:
  0.6 0.0 copy-start
  0.7 1.5 %constant_dynamic-slice_fusion = f32[1,2048]{1,0:T(1,128)} fusion(f32[4,2048]{1,0:T(4,128)} %param.20, s32[]{:T(128)S(6)} %select_n.22), kind=kLoop, calls=%fused_computation.31 | loop fusion | bytes 16388 | tf_op jit(solution)/shard_map/dynamic_slice | solution.py:528
  2.1 0.7 convert_element_type.39
  2.8 1.5 %fusion = f32[256]{0:T(256)S(1)} fusion(bf16[256,2048]{1,0:T(8,128)(2,1)} %param.15), kind=kLoop, calls=%fused_computation.2 | loop fusion | flops 1572608 | bytes 1049600 | tf_op jit(solution)/shard_map/reduce_sum | solution.py:18
  4.3 0.0 copy-done
  4.3 0.0 copy-start.4
  4.3 0.0 copy-start.3
  4.4 1.8 %fusion.4 = bf16[256,256]{1,0:T(8,128)(2,1)S(1)} fusion(bf16[256,2048]{1,0:T(8,128)(2,1)S(1)} %copy-done, bf16[256,2048]{1,0:T(8,128)(2,1)} %param.15, f32[2048]{0:T(1024)S(1)} %convert_element_type.39, f32[256]{0:T(256)S(1)} %add_rsqrt_fusion), kind=kOutput, calls=%fused_computation.11 | convolution fusion | flops 270663680 | bytes 2237440 | tf_op jit(solution)/shard_map/dot_general | solution.py:23
  6.1 0.0 copy-start.1
  6.1 0.1 copy.33
  6.3 0.2 copy.34
  6.5 0.8 pad_maximum_fusion.1.q_ref
  7.2 0.0 copy-done.4
  7.3 0.0 copy-start.8
  7.3 0.2 convolution_convert_fusion.4
  7.5 0.1 eq.40
  7.6 0.2 fusion.8
  7.7 0.0 copy-done.3
  7.7 1.1 %convolution_convert_fusion = bf16[512,512]{1,0:T(8,128)(2,1)} fusion(pred[96,512]{0,1:T(32,128)(4,1)S(1)} %fusion.8, bf16[96,512]{1,0:T(8,128)(2,1)S(1)} %copy-done.3), kind=kOutput, calls=%fused_computation.5 | convolution fusion | flops 50593792 | bytes 671744 | tf_op jit(solution)/shard_map/dot_general | solution.py:543
  8.8 0.0 copy-done.1
  8.8 1.8 %convolution_convert_fusion.3 = bf16[256,256]{0,1:T(8,128)(2,1)S(1)} fusion(bf16[256,2048]{1,0:T(8,128)(2,1)} %param.18, bf16[256,2048]{1,0:T(8,128)(2,1)S(1)} %copy-done.1, f32[2048]{0:T(1024)S(1)} %convert_element_type.39, f32[256]{0:T(256)S(1)} %add_rsqrt_fusion), kind=kOutput, calls=%fused_computation.9 | convolution fusion | flops 270598144 | bytes 2237440 | tf_op jit(solution)/shard_map/dot_general | solution.py:23
  10.7 0.0 copy-done.8
  10.7 0.0 copy-start.7
  10.7 0.0 copy-start.5
  10.7 0.6 convolution_convert_fusion.2
  11.3 0.8 copy.32
  12.2 0.0 copy-done.7
  12.2 0.6 broadcast_in_dim.53.gain_ref
  12.8 0.0 copy-done.5
  12.8 0.6 broadcast_in_dim.54.mix_gain
  13.4 0.0 copy-start.6
  13.4 73.4 %shard_map.158 = (bf16[256,2048]{1,0:T(8,128)(2,1)}, bf16[512,512]{1,0:T(8,128)(2,1)}) custom-call(bf16[4,256,128]{2,1,0:T(8,128)(2,1)} %bitcast.55, bf16[8,64,128]{2,1,0:T(8,128)(2,1)} %pad_maximum_fusion.1.q_ref, f32[8,1,256]{2,1,0:T(1,128)} %bitcast.61, bf16[8,64,512]{2,1,0:T(8,128)(2,1)} %bitcast.51, bf16[16,512]{1,0:T(8,128)(2,1)} %broadcast_in_dim.53.gain_ref, ...), custom_call_target="tpu_custom_call" | custom-call | tf_op jit(solution)/shard_map/pallas_call | solution.py:465
  86.8 0.0 copy-start.2
  86.8 0.0 copy-done.6
  86.8 0.1 fusion.6
  87.0 1.4 %fusion.21 = f32[96,512]{1,0:T(8,128)S(1)} fusion(bf16[96,512]{0,1:T(8,128)(2,1)S(1)} %fusion.6, bf16[512,512]{1,0:T(8,128)(2,1)} %get-tuple-element.5), kind=kOutput, calls=%fused_computation.35 | convolution fusion | flops 50331648 | bytes 819200 | tf_op jit(solution)/shard_map/dot_general | solution.py:563
  88.4 0.1 fusion.7
  88.5 1.9 %fusion.3 = bf16[96,512]{1,0:T(8,128)(2,1)} fusion(f32[96,512]{1,0:T(8,128)S(1)} %fusion.21, bf16[96,512]{0,1:T(8,128)(2,1)S(1)} %fusion.7, bf16[512,512]{1,0:T(8,128)(2,1)} %get-tuple-element.5), kind=kOutput, calls=%fused_computation.10 | convolution fusion | flops 50429952 | bytes 917504 | tf_op jit(solution)/shard_map/dot_general | solution.py:563
  90.4 0.0 copy-done.2
  90.4 1.0 %copy.38 = bf16[256,2048]{1,0:T(8,128)(2,1)} copy(bf16[256,2048]{1,0:T(8,128)(2,1)S(1)} %copy-done.2) | data formatting | bytes 2097152
  (8 shorter events, 0.1 us)
Async XLA Ops:
  0.6 3.7 %copy-start = (bf16[256,2048]{1,0:T(8,128)(2,1)S(1)}, bf16[256,2048]{1,0:T(8,128)(2,1)}, u32[]{:S(2)}) copy-start(bf16[256,2048]{1,0:T(8,128)(2,1)} %param.17) | copy-start | bytes 3145732
  4.3 2.9 %copy-start.4 = (s32[96,4]{0,1:T(4,128)S(1)}, s32[96,4]{0,1:T(4,128)}, u32[]{:S(2)}) copy-start(s32[96,4]{0,1:T(4,128)} %param.25) | copy-start | bytes 4612
  4.3 3.4 %copy-start.3 = (bf16[96,512]{1,0:T(8,128)(2,1)S(1)}, bf16[96,512]{1,0:T(8,128)(2,1)}, u32[]{:S(2)}) copy-start(bf16[96,512]{1,0:T(8,128)(2,1)} %param.23) | copy-start | bytes 294916
  6.1 2.7 %copy-start.1 = (bf16[256,2048]{1,0:T(8,128)(2,1)S(1)}, bf16[256,2048]{1,0:T(8,128)(2,1)}, u32[]{:S(2)}) copy-start(bf16[256,2048]{1,0:T(8,128)(2,1)} %param.15) | copy-start | bytes 3145732
  7.3 3.4 %copy-start.8 = (bf16[256,2048]{1,0:T(8,128)(2,1)S(1)}, bf16[256,2048]{1,0:T(8,128)(2,1)}, u32[]{:S(2)}) copy-start(bf16[256,2048]{1,0:T(8,128)(2,1)} %param.19) | copy-start | bytes 3145732
  10.7 1.5 %copy-start.7 = (bf16[512]{0:T(512)(128)(2,1)S(1)}, bf16[512]{0:T(512)(128)(2,1)}, u32[]{:S(2)}) copy-start(bf16[512]{0:T(512)(128)(2,1)} %param.24) | copy-start | bytes 3076
  10.7 2.1 %copy-start.5 = (bf16[2048]{0:T(1024)(128)(2,1)S(1)}, bf16[2048]{0:T(1024)(128)(2,1)}, u32[]{:S(2)}) copy-start(bf16[2048]{0:T(1024)(128)(2,1)} %param.22) | copy-start | bytes 12292
  13.4 73.4 %copy-start.6 = (f32[96,4]{0,1:T(4,128)S(1)}, f32[96,4]{0,1:T(4,128)}, u32[]{:S(2)}) copy-start(f32[96,4]{0,1:T(4,128)} %param.26) | copy-start | bytes 4612
  86.8 3.7 %copy-start.2 = (bf16[256,2048]{1,0:T(8,128)(2,1)S(1)}, bf16[256,2048]{1,0:T(8,128)(2,1)}, u32[]{:S(2)}) copy-start(bf16[256,2048]{1,0:T(8,128)(2,1)} %get-tuple-element.10) | copy-start | bytes 3145732
where the time goes:
time: 91.8 us; the launch traced here: 91.4 us
  Pallas kernels  73.4 us (80%)
  matrix products  8.8 us (10%)
  local copies, waits for them, and re-layouts  4.93 us (5%)
  other arithmetic  3.45 us (4%)
    pallas_call x1, Pallas kernels, one_call(): pl.pallas_call(functools.partial(kernel, (ep, tp, share, part, packed)),...  73.4 us
    dot_general x3, matrix products, project(): lax.dot_general(normed, weight, (((1,), (1,)), ((), ())), preferred_eleme...  4.19 us
    dot_general x2, matrix products, on_device(): lax.dot_general(part_of, returned, (((1,), (0,)), ((), ())), preferred_el...  3.32 us

commit v1 on v0

--- a/solution.py
+++ b/solution.py
@@ -20,10 +20,9 @@
 
 
 def project(normed, weight):
-    product = lax.dot_general(
+    return lax.dot_general(
         normed, weight, (((1,), (1,)), ((), ())), preferred_element_type=jnp.float32
     )
-    return product.astype(jnp.bfloat16)
 
 
 def gated_units(gate_pre, up_pre):
@@ -49,22 +48,27 @@
 
 
 def kernel(
-    dims, kv_ref, q_ref, off_ref, exp_ref, gain_ref, wg_hbm, wu_hbm, wd_hbm, wo_hbm, mix_gain,
-    out_ref, ret_ref,
+    dims, routes_ref, scale_ref, gains_ref, off_ref, exp_ref, mix_hbm, wq_hbm, wk_hbm, wv_hbm,
+    wg_hbm, wu_hbm, wd_hbm, wo_hbm,
+    out_ref, exp_out_ref,
+    mix_ref, normed_ref, wq_ref, wkv_ref, kv_ref, q_ref, x_out, key_ref, weight_ref, ret_ref,
     kv_all, q_all, seg_ref, wg_ref, wu_ref, wd_ref, wo_ref, sum_ref, e_got, e_pair, e_y, e_fin,
     att_ref, att_all, att_rows, m_send, m_got, m_sum,
-    kv_send, kv_recv, q_send, q_recv, x_send, x_recv, p_send, p_recv, g_send, g_recv,
+    kv_send, kv_recv, k_send, q_send, q_recv, x_send, x_recv, p_send, p_recv, g_send, g_recv,
     f_send, f_recv, d_send, d_recv, y_send, y_recv, z_send, z_recv, a_send, a_recv,
-    h_send, h_recv, v_send, v_recv, o_send, o_recv, own_sem, w_sem,
+    h_send, h_recv, v_send, v_recv, o_send, o_recv, mix_sem, w_sem,
 ):
-    ep, tp, share, part, packed = dims
+    ep, tp, share, part, packed, cap = dims
     chips = tp // 2
     heads = ep // share
     me = lax.axis_index("ep")
     mt = lax.axis_index("tp")
     core = lax.rem(mt, 2)
     partner = mt + 1 - 2 * core
-    cap, width = exp_ref.shape[1:]
+    token_count, width = exp_ref.shape
+    full = seg_ref.shape[1]
+    head_size = wk_hbm.shape[0] // heads
+    tail_rows = seg_ref.shape[0] - ep * cap
     block = kv_ref.shape[1]
     half = out_ref.shape[0] // 2
     pieces = o_send.shape[0]
@@ -81,6 +85,18 @@
     def other(k):
         return lax.rem(mt + 2 * k, tp)
 
+    stride = head_size if packed else 2 * head_size
+    places = [(mix_hbm, mix_ref)]
+    for h in range(heads):
+        one = pl.ds(h * head_size, head_size)
+        places.append((wk_hbm.at[one], wkv_ref.at[pl.ds(2 * h * head_size, head_size)]))
+        places.append((wv_hbm.at[one], wkv_ref.at[pl.ds((2 * h + 1) * head_size, head_size)]))
+        places.append((wq_hbm.at[one], wq_ref.at[pl.ds(h * stride, head_size)]))
+    mix_loads = [
+        pltpu.make_async_copy(src, dst, mix_sem.at[i]) for i, (src, dst) in enumerate(places)
+    ]
+    for copy in mix_loads:
+        copy.start()
     weights = [
         pltpu.make_async_copy(src, dst, w_sem.at[i])
         for i, (src, dst) in enumerate(
@@ -100,7 +116,6 @@
     pl.semaphore_signal(barrier, inc=1, device_id={"tp": partner}, device_id_type=MESH)
     for k in range(1, chips):
         pl.semaphore_signal(barrier, inc=1, device_id={"tp": other(k)}, device_id_type=MESH)
-    pl.semaphore_wait(barrier, ep - 1 + 1 + chips - 1)
 
     def remote(src, dst, send, recv, where):
         return pltpu.make_async_remote_copy(
@@ -116,7 +131,7 @@
 
     def x_copy(s):
         return remote(
-            exp_ref.at[peer(s)], seg_ref.at[rows(s), columns(mt)], x_send.at[s], x_recv.at[s],
+            x_out.at[s], seg_ref.at[rows(s), columns(mt)], x_send.at[s], x_recv.at[s],
             {"ep": peer(s)},
         )
 
@@ -126,29 +141,53 @@
             {"ep": dest},
         )
 
+    def k_copy(slot):
+        return remote(
+            kv_all.at[slot], kv_all.at[slot], k_send.at[slot], kv_recv.at[slot], {"ep": twin}
+        )
+
     def q_copy(dest, slot):
         return remote(
             q_ref.at[dest], q_all.at[slot], q_send.at[dest], q_recv.at[slot], {"ep": dest}
         )
 
-    tail = pl.ds(ep * cap, gain_ref.shape[0])
-    own_x = pltpu.make_async_copy(exp_ref.at[me], seg_ref.at[rows(0), columns(mt)], own_sem.at[2])
-    own_g = pltpu.make_async_copy(gain_ref, seg_ref.at[tail, columns(mt)], own_sem.at[3])
-    own_kv = pltpu.make_async_copy(kv_ref.at[me // share], kv_all.at[me], own_sem.at[0])
-    own_q = pltpu.make_async_copy(q_ref.at[me], q_all.at[me], own_sem.at[1])
-    for copy in (own_x, own_g, own_kv, own_q):
-        copy.start()
+    tail = pl.ds(ep * cap, tail_rows)
+    step = 2 if share % 2 == 0 else 1
+    twin = me + 1 - 2 * lax.rem(me, 2)
+
+    expert_ids = lax.broadcasted_iota(jnp.int32, (ep, token_count), 0)
+    chosen = jnp.zeros((ep, token_count), jnp.float32)
+    weight = jnp.zeros((ep, token_count), jnp.float32)
+    for k in range(routes_ref.shape[0]):
+        hit = routes_ref[k : k + 1, :] == expert_ids
+        chosen = jnp.where(hit, 1.0, chosen)
+        weight = jnp.where(hit, scale_ref[k : k + 1, :], weight)
+    earlier = (
+        lax.broadcasted_iota(jnp.int32, (token_count, token_count), 0)
+        < lax.broadcasted_iota(jnp.int32, (token_count, token_count), 1)
+    ).astype(jnp.float32)
+    slot_of = jnp.dot(chosen, earlier, preferred_element_type=jnp.float32)
+    key_ref[...] = jnp.where(chosen > 0.0, slot_of, -1.0)
+    weight_ref[...] = weight
+    slot_ids = lax.broadcasted_iota(jnp.int32, (cap, token_count), 0).astype(jnp.float32)
+
+    def placed(e):
+        return key_ref[pl.ds(e, 1), :] == slot_ids
+
+    def routed(s):
+        picked = jnp.where(placed(peer(s)), 1.0, 0.0).astype(jnp.bfloat16)
+        return jnp.dot(picked, exp_ref[...], preferred_element_type=jnp.float32).astype(
+            jnp.bfloat16
+        )
+
+    for s in range(1, ep):
+        x_out[s] = routed(s)
+    pl.semaphore_wait(barrier, ep - 1 + 1 + chips - 1)
     for s in range(1, ep):
         x_copy(s).start()
-
-    def send_mix(s, _):
-        q_copy(peer(s), me).start()
-        kv_copy(peer(s), me).start()
-        return 0
-
-    lax.fori_loop(1, ep, send_mix, 0)
-    for copy in (own_x, own_g, own_kv, own_q):
-        copy.wait()
+    exp_gain = gains_ref[:, 2 * full :]
+    seg_ref[tail, columns(mt)] = jnp.broadcast_to(exp_gain, (tail_rows, width)).astype(jnp.bfloat16)
+    seg_ref[rows(0), columns(mt)] = routed(0)
 
     def rows_of(n):
         return tail if n == ep else rows(n)
@@ -231,9 +270,7 @@
                 y_copy(k, s).start()
         d_copy(0, g).wait_recv()
 
-    own_fin = pltpu.make_async_copy(
-        e_fin.at[rows(0)], ret_ref.at[pl.ds(pl.multiple_of(me * cap, cap), cap)], own_sem.at[4]
-    )
+    early = ep // 2 - 1
 
     def fin(s):
         total = sum_ref[rows(s), columns(mt)].astype(jnp.float32)
@@ -241,26 +278,83 @@
         for k in range(1, chips):
             y_copy(k, s).wait_recv()
             total = total + e_y[k - 1, rows(s), :].astype(jnp.float32)
-        e_fin[rows(s), :] = total.astype(jnp.bfloat16)
         if s > 0:
+            e_fin[rows(s), :] = total.astype(jnp.bfloat16)
+        else:
+            ret_ref[pl.ds(pl.multiple_of(me * cap, cap), cap), :] = total.astype(jnp.bfloat16)
+        if 0 < s <= early:
             z_copy(s).start()
-        else:
-            own_fin.start()
 
     spread(ep)
+    spread(0)
+
+    def send_mix():
+        for copy in mix_loads:
+            copy.wait()
+        gain = gains_ref[:, :full]
+        chunk = min(64, block)
+        for r in range(0, block, chunk):
+            at = pl.ds(r, chunk)
+            normed_ref[at, :] = normalize(mix_ref[at, :].astype(jnp.float32), gain).astype(
+                jnp.bfloat16
+            )
+        if not packed:
+            for h in range(heads):
+                at = pl.ds(h * stride + head_size, head_size)
+                wq_ref[at, :] = jnp.zeros((head_size, full), jnp.bfloat16)
+        both = project(normed_ref[...], wkv_ref[...])
+        for h in range(heads):
+            kv_ref[h] = both[:, h * 128 : (h + 1) * 128].astype(jnp.bfloat16)
+        kv_all[me] = kv_ref[me // share]
+        for i in range(step, ep, step):
+            dest = lax.rem(me + i, ep)
+            kv_copy(dest, me).start()
+        if step == 2:
+            k_copy(me).start()
+        q = project(normed_ref[...], wq_ref[...]) * (1.0 / math.sqrt(head_size))
+        for r in range(share):
+            one = q[r * part : (r + 1) * part]
+            if packed:
+                first, second = one[: part // 2], one[part // 2 :]
+                for h in range(0, heads, 2):
+                    at = slice(h * head_size, (h + 2) * head_size)
+                    left, right = first[:, at], second[:, at]
+                    even = jnp.where(lane < 64, left, pltpu.roll(right, 64, 1))
+                    odd = jnp.where(lane < 64, pltpu.roll(left, 64, 1), right)
+                    q_ref[h * share + r] = even.astype(jnp.bfloat16)
+                    q_ref[(h + 1) * share + r] = odd.astype(jnp.bfloat16)
+            else:
+                for h in range(heads):
+                    q_ref[h * share + r] = one[:, h * 128 : (h + 1) * 128].astype(jnp.bfloat16)
+        q_all[me] = q_ref[me]
+
+        def send_q(s, _):
+            q_copy(peer(s), me).start()
+            return 0
+
+        lax.fori_loop(1, ep, send_q, 0)
+
+    def pass_on(i):
+        slot = lax.rem(me - i + ep, ep)
+        kv_copy(peer(1), slot).wait_recv()
+        k_copy(slot).start()
+
+    lane = lax.broadcasted_iota(jnp.int32, (1, 128), 1)
+    send_mix()
+    for n in range(1, ep):
+        spread(n)
+        if n == 1:
+            forward(ep)
+            forward(0)
+        if n >= 3:
+            forward(n - 2)
+    if ep == 1:
+        forward(ep)
+        forward(0)
+    for n in range(max(1, ep - 2), ep):
+        forward(n)
     for g in range(groups):
-        lag = 2
         first, last = g * per, (g + 1) * per
-        for s in range(first, last):
-            spread(s)
-            if s == 1:
-                forward(ep)
-            if s - lag >= first:
-                forward(s - lag)
-        if ep == 1:
-            forward(ep)
-        for s in range(max(first, last - lag), last):
-            forward(s)
         if g == 0:
             gathered(ep)
             for copy in weights:
@@ -270,13 +364,15 @@
         for s in range(first, last):
             gathered(s)
         expert(g)
+    if step == 2:
+        for i in range(2, ep, 2):
+            pass_on(i)
 
     def q_wait(s, _):
         q_copy(peer(s), before(s)).wait_recv()
         return 0
 
     lax.fori_loop(1, ep, q_wait, 0)
-    lane = lax.broadcasted_iota(jnp.int32, (1, 128), 1)
 
     def queries(i):
         both = q_all[i].astype(jnp.float32)
@@ -295,12 +391,12 @@
     for n in range(ep):
         j = ep - 1 - n
 
-        @pl.when(me != j)
+        @pl.when((me != j) if step == 1 else (lax.rem(me, 2) != j % 2))
         def _():
-            kv_copy(lax.rem(2 * me - j + ep, ep), j).wait_recv()
+            kv_copy(peer(1), j).wait_recv()
 
         kv = kv_all[j]
-        off = off_ref[j]
+        off = off_ref[pl.ds(me // share, 1), j * block : (j + 1) * block]
         q = queries(j)
         zero_carry = jnp.zeros((part, 1), jnp.float32)
         zero_acc = jnp.zeros((part, 128), jnp.float32)
@@ -336,11 +432,11 @@
         return 0
 
     lax.fori_loop(1, ep, start_a, 0)
-    own_att = pltpu.make_async_copy(att_ref.at[me], att_all.at[me], own_sem.at[5])
-    own_att.start()
+    att_all[me] = att_ref[me]
     for s in range(done, ep):
         fin(s)
-    own_att.wait()
+    for s in range(early + 1, ep):
+        z_copy(s).start()
 
     def wait_a(s, _):
         a_copy(peer(s), before(s)).wait_recv()
@@ -349,7 +445,7 @@
     lax.fori_loop(1, ep, wait_a, 0)
     for r in range(share):
         got = [att_all[h * share + r].astype(jnp.float32) for h in range(heads)]
-        if packed and heads % 2 == 0:
+        if packed:
             upper = []
             lower = []
             for h in range(0, heads, 2):
@@ -361,10 +457,7 @@
         else:
             both = []
             for h in range(heads):
-                whole = got[h]
-                if packed:
-                    whole = jnp.concatenate([pltpu.roll(whole, 64, 1), whole], axis=0)
-                both.append(jnp.where(lane < 64, 0.0, whole))
+                both.append(jnp.where(lane < 64, 0.0, got[h]))
             both = jnp.concatenate(both, axis=1)
         att_rows[pl.ds(r * part, part), :] = both.astype(jnp.bfloat16)
 
@@ -397,9 +490,28 @@
         at = out_ref.at[pl.ds(pl.multiple_of(core * half + i * piece, piece), piece)]
         return remote(at, at, o_send.at[i], o_recv.at[i], {"tp": partner})
 
-    gain = mix_gain[...].astype(jnp.float32)
+    gain = gains_ref[:, full : 2 * full]
+
+    def combine():
+        total = jnp.zeros((token_count, width), jnp.float32)
+        for s in range(ep):
+            if s > 0:
+                z_arrived(s).wait_recv()
+            e = peer(s)
+            spread_to = jnp.where(placed(e), weight_ref[pl.ds(e, 1), :], 0.0)
+            high = spread_to.astype(jnp.bfloat16).astype(jnp.float32)
+            both = jnp.concatenate([high, spread_to - high], axis=0).T.astype(jnp.bfloat16)
+            got = ret_ref[pl.ds(pl.multiple_of(e * cap, cap), cap), :]
+            for low in range(2):
+                total = total + jnp.dot(
+                    both[:, low * cap : (low + 1) * cap], got, preferred_element_type=jnp.float32
+                )
+        exp_out_ref[...] = total.astype(jnp.bfloat16)
+
     for i in range(pieces):
         at = pl.ds(i * piece, piece)
+        if i == min(2, pieces - 1):
+            combine()
         for k in range(1, chips):
             v_copy(k, i).wait_recv()
         total = jnp.zeros((piece, out_ref.shape[1]), jnp.float32)
@@ -410,7 +522,6 @@
         out_ref[own_rows, :] = normalize(total, gain).astype(jnp.bfloat16)
         o_copy(i).start()
 
-    own_fin.wait()
     h_copy.wait_send()
     for n in range(ep + 1):
         p_copy(n).wait_send()
@@ -428,30 +539,40 @@
     for s in range(1, ep):
         x_copy(s).wait_send()
         z_copy(s).wait_send()
-        z_arrived(s).wait_recv()
 
     def finish(s, _):
         q_copy(peer(s), me).wait_send()
-        kv_copy(peer(s), me).wait_send()
         a_copy(peer(s), me).wait_send()
         return 0
 
     lax.fori_loop(1, ep, finish, 0)
+    for i in range(step, ep, step):
+        kv_copy(lax.rem(me + i, ep), me).wait_send()
+    if step == 2:
+        for i in range(0, ep, 2):
+            k_copy(lax.rem(me - i + ep, ep)).wait_send()
     for i in range(pieces):
         at = out_ref.at[pl.ds(pl.multiple_of((1 - core) * half + i * piece, piece), piece)]
         remote(at, at, o_send.at[i], o_recv.at[i], {"tp": partner}).wait_recv()
         o_copy(i).wait_send()
 
 
-def one_call(ep, tp, share, part, packed, kv, q, off, outgoing, gain, wg, wu, wd, wo, out_gain):
-    cap, width = outgoing.shape[1:]
-    slots, full = ep * cap, tp * width
+def one_call(
+    ep, tp, share, part, packed, cap, routes, scale, gains, off, exp_rows, mix, wq, wk, wv,
+    wg, wu, wd, wo,
+):
+    token_count, width = exp_rows.shape
+    row_count, full = mix.shape
+    heads = off.shape[0]
+    head_size = wq.shape[0] // heads
+    slots = ep * cap
     chips = tp // 2
-    row_count = share * part
     half = row_count // 2
     pieces = 4
     groups = 2 if ep % 2 == 0 else 1
     others = max(chips - 1, 1)
+    q_rows = part // 2 if packed else part
+    q_stride = head_size if packed else 2 * head_size
     dma = pltpu.SemaphoreType.DMA
     vmem = pl.BlockSpec(memory_space=pltpu.VMEM)
     hbm = pl.BlockSpec(memory_space=pl.ANY)
@@ -463,29 +584,34 @@
         return [dma(shape), dma(shape)]
 
     return pl.pallas_call(
-        functools.partial(kernel, (ep, tp, share, part, packed)),
+        functools.partial(kernel, (ep, tp, share, part, packed, cap)),
         out_shape=(
             jax.ShapeDtypeStruct((row_count, full), jnp.bfloat16),
-            jax.ShapeDtypeStruct((slots, width), jnp.bfloat16),
+            jax.ShapeDtypeStruct((token_count, width), jnp.bfloat16),
         ),
-        in_specs=[vmem] * 5 + [hbm] * 4 + [vmem],
+        in_specs=[vmem] * 5 + [hbm] * 8,
         out_specs=(vmem, vmem),
         scratch_shapes=[
-            held(ep, *kv.shape[1:]), held(ep, *q.shape[1:]),
-            held(slots + gain.shape[0], full),
+            held(row_count, full), held(row_count, full), held(heads * q_stride, full),
+            held(2 * heads * head_size, full), held(heads, row_count, 128),
+            held(ep, q_rows, 128), held(ep, cap, width),
+            pltpu.VMEM((ep, token_count), jnp.float32), pltpu.VMEM((ep, token_count), jnp.float32),
+            held(slots, width),
+            held(ep, row_count, 128), held(ep, q_rows, 128),
+            held(slots + 16, full),
             held(*wg.shape), held(*wu.shape), held(*wd.shape), held(*wo.shape),
             held(slots, full), held(chips, slots, width), held(others, slots, width),
             held(others, slots, width), held(slots, width),
-            held(*q.shape), held(*q.shape), held(row_count, wo.shape[0]),
+            held(ep, q_rows, 128), held(ep, q_rows, 128), held(row_count, wo.shape[0]),
             held(half, full), held(half, full), held(chips, half, full),
         ]
-        + both(ep) + both(ep) + both(ep) + both(ep + 1) + both(chips, ep + 1)
+        + both(ep) + [dma((ep,))] + both(ep) + both(ep) + both(ep + 1) + both(chips, ep + 1)
         + both(chips, ep + 1) + both(chips, groups) + both(chips, ep) + both(ep) + both(ep)
-        + both(1) + both(chips, pieces) + both(pieces) + [dma((6,)), dma((4,))],
+        + both(1) + both(chips, pieces) + both(pieces) + [dma((1 + 3 * heads,)), dma((4,))],
         compiler_params=pltpu.CompilerParams(
             collective_id=0, has_side_effects=True, vmem_limit_bytes=60 * 1024 * 1024
         ),
-    )(kv, q, off, outgoing, gain, wg, wu, wd, wo, out_gain)
+    )(routes, scale, gains, off, exp_rows, mix, wq, wk, wv, wg, wu, wd, wo)
 
 
 def on_device(
@@ -512,59 +638,19 @@
     head_size = w_query.shape[0] // heads_here
     share = ep // heads_here
     part = row_count // share
-    packed = part % 32 == 0
-    normed = normalize(mix_rows.astype(jnp.float32), mix_gain).astype(jnp.bfloat16)
-    queries = project(normed, w_query) * jnp.bfloat16(1.0 / math.sqrt(head_size))
-    keys = project(normed, w_key).reshape(row_count, heads_here, 1, head_size)
-    values = project(normed, w_value).reshape(row_count, heads_here, 1, head_size)
-    kv = jnp.concatenate([keys, values], axis=2).reshape(row_count, heads_here, 2 * head_size)
-    kv = kv.transpose(1, 0, 2)
-    q = queries.reshape(share, part, heads_here, head_size).transpose(2, 0, 1, 3)
-    q = q.reshape(ep, part, head_size)
-    if packed:
-        q = jnp.concatenate([q[:, : part // 2], q[:, part // 2 :]], axis=2)
-    else:
-        q = jnp.concatenate([q, jnp.zeros_like(q)], axis=2)
-    off = lax.dynamic_slice_in_dim(key_offset, lax.axis_index("ep") // share, 1, 0)
-    off = off.reshape(ep, 1, row_count)
-
+    packed = part % 32 == 0 and heads_here % 2 == 0
     token_count, top_count = routes.shape
     experts = w_gate.shape[0] * ep
     capacity = 4 * token_count * top_count // (3 * experts)
-    named = routes[:, :, None] == jnp.arange(experts, dtype=jnp.int32)
-    chosen = jnp.any(named, axis=1)
-    weight = jnp.sum(jnp.where(named, route_weight[:, :, None], 0.0), axis=1)
-    before = jnp.tril(jnp.ones((token_count, token_count), jnp.bfloat16), -1)
-    slot = jnp.dot(before, chosen.astype(jnp.bfloat16), preferred_element_type=jnp.float32)
-    placed = chosen[:, :, None] & (
-        slot.astype(jnp.int32)[:, :, None] == jnp.arange(capacity, dtype=jnp.int32)
-    )
-    flat = placed.reshape(token_count, experts * capacity)
-    outgoing = lax.dot_general(
-        flat.astype(jnp.bfloat16), exp_rows, (((0,), (0,)), ((), ())),
-        preferred_element_type=jnp.float32,
-    ).astype(jnp.bfloat16)
-    outgoing = outgoing.reshape(experts, capacity, -1)
-    gain = jnp.broadcast_to(exp_gain[None], (16, exp_gain.shape[0]))
-
-    slots = experts * capacity
-    if not (packed and heads_here % 2 == 0):
+    gains = jnp.concatenate([mix_gain, out_gain, exp_gain]).astype(jnp.float32)[None]
+    if not packed:
         w_out = w_out.reshape(heads_here, head_size, -1)
         w_out = jnp.concatenate([jnp.zeros_like(w_out), w_out], axis=1)
         w_out = w_out.reshape(2 * heads_here * head_size, -1)
-    mix_out, returned = one_call(
-        ep, tp, share, part, packed, kv, q, off, outgoing, gain,
-        w_gate[0], w_up[0], w_down[0], w_out, out_gain[None],
+    mix_out, exp_out = one_call(
+        ep, tp, share, part, packed, capacity, routes.T, route_weight.T, gains, key_offset,
+        exp_rows, mix_rows, w_query, w_key, w_value, w_gate[0], w_up[0], w_down[0], w_out,
     )
-    spread = jnp.where(placed, weight[:, :, None], 0.0).reshape(token_count, slots)
-    high = spread.astype(jnp.bfloat16)
-    low = (spread - high.astype(jnp.float32)).astype(jnp.bfloat16)
-    exp_out = sum(
-        lax.dot_general(
-            part_of, returned, (((1,), (0,)), ((), ())), preferred_element_type=jnp.float32
-        )
-        for part_of in (high, low)
-    ).astype(jnp.bfloat16)
     return (mix_out, exp_out)
 
 

time: 91.8 us -> 76.8 us (0.84)
  matrix products: 8.8 us -> 0 us
  Pallas kernels: 73.4 us -> 70.2 us
  other arithmetic: 3.45 us -> 0.63 us
    dot_general x7 -> x0, matrix products: 8.8 us -> none  [the longest x3 4.19 us: project(): lax.dot_general(normed, weight, (((1,), (1,)), ((), ())), preferred_eleme...]
    pallas_call x1, Pallas kernels: 73.4 us -> 70.2 us  [one_call(): pl.pallas_call(functools.partial(kernel, (ep, tp, share, part, packed, ca...]
    concatenate x0 -> x3, local copies, waits for them, and re-layouts: none -> 2.07 us  [on_device(): jnp.concatenate([mix_gain, out_gain, exp_gain]).astype(jnp.float32)[None]]
    unnamed x19 -> x4, local copies, waits for them, and re-layouts: 1.02 us -> 2.98 us
    reduce_sum x2 -> x0, other arithmetic: 1.52 us -> none  [the longest x1 1.51 us: normalize(): jnp.mean(numbers * numbers, axis=-1, keepdims=True) + EPSILON]
    dynamic_slice x1 -> x0, local copies, waits for them, and re-layouts: 1.45 us -> none  [on_device(): lax.dynamic_slice_in_dim(key_offset, lax.axis_index('ep') // share, 1, 0)]
    broadcast_in_dim x2 -> x0, local copies, waits for them, and re-layouts: 1.2 us -> none  [the longest x1 0.61 us: on_device(): gain = jnp.broadcast_to(exp_gain[None], (16, exp_gain.shape[0]))]
where the time goes in v1:
time: 76.8 us; the launch traced here: 76.6 us
  Pallas kernels  70.2 us (91%)
  local copies, waits for them, and re-layouts  5.05 us (7%)
    pallas_call x1, Pallas kernels, one_call(): pl.pallas_call(functools.partial(kernel, (ep, tp, share, part, packed, ca...  70.2 us
    unnamed x4, local copies, waits for them, and re-layouts  2.98 us
    concatenate x3, local copies, waits for them, and re-layouts, on_device(): jnp.concatenate([mix_gain, out_gain, exp_gain]).astype(jnp.float32)[None]  2.07 us

profile of v1, /device:TPU:0, one launch (start us, length us, event | category | flops | bytes accessed | tf_op | source)
XLA Modules:
  0.0 76.6 jit_solution(9209917484195129972)
XLA Ops:
  0.6 0.7 concatenate.18
  1.3 0.7 concatenate.16
  2.0 0.7 concatenate.17
  2.7 0.6 maximum_convert_fusion.gains_ref
  3.3 70.2 %shard_map.158 = (bf16[256,2048]{1,0:T(8,128)(2,1)}, bf16[96,512]{1,0:T(8,128)(2,1)}) custom-call(s32[4,96]{1,0:T(4,128)} %bitcast.8, f32[4,96]{1,0:T(4,128)} %bitcast.9, f32[1,4608]{1,0:T(1,128)} %maximum_convert_fusion.gains_ref, f32[4,2048]{1,0:T(4,128)} %off_ref.1, bf16[96,512]{1,0:T(8,128)(2,1)} %exp_ref.1, bf16[256,2048]{1,0:T(8,128)(2,1)} %mix_hbm.1, ...), custom_call_target="tpu_custom_call" | custom-call | tf_op jit(solution)/shard_map/pallas_call | solution.py:586
  73.6 0.0 copy-start
  73.6 2.3 %copy.19 = bf16[256,2048]{1,0:T(8,128)(2,1)} copy(bf16[256,2048]{1,0:T(8,128)(2,1)} %get-tuple-element.4) | data formatting | bytes 2097152
  75.9 0.0 copy-done
  75.9 0.6 copy.20
Async XLA Ops:
  73.6 2.4 %copy-start = (bf16[96,512]{1,0:T(8,128)(2,1)S(1)}, bf16[96,512]{1,0:T(8,128)(2,1)}, u32[]{:S(2)}) copy-start(bf16[96,512]{1,0:T(8,128)(2,1)} %get-tuple-element.5) | copy-start | bytes 294916

commit v2 on v1

--- a/solution.py
+++ b/solution.py
@@ -53,10 +53,11 @@
     out_ref, exp_out_ref,
     mix_ref, normed_ref, wq_ref, wkv_ref, kv_ref, q_ref, x_out, key_ref, weight_ref, ret_ref,
     kv_all, q_all, seg_ref, wg_ref, wu_ref, wd_ref, wo_ref, sum_ref, e_got, e_pair, e_y, e_fin,
-    att_ref, att_all, att_rows, m_send, m_got, m_sum,
+    att_ref, att_all, att_rows, m_send, m_got, m_sum, att_wide,
     kv_send, kv_recv, k_send, q_send, q_recv, x_send, x_recv, p_send, p_recv, g_send, g_recv,
     f_send, f_recv, d_send, d_recv, y_send, y_recv, z_send, z_recv, a_send, a_recv,
-    h_send, h_recv, v_send, v_recv, o_send, o_recv, mix_sem, w_sem,
+    h_send, h_recv, v_send, v_recv, o_send, o_recv, b_send, b_recv, wy_send, wy_recv,
+    wx_send, wx_recv, wd_send, wd_recv, mix_sem, w_sem,
 ):
     ep, tp, share, part, packed, cap = dims
     chips = tp // 2
@@ -75,6 +76,11 @@
     piece = half // pieces
     groups = d_send.shape[1]
     per = ep // groups
+    channels = wo_hbm.shape[0]
+    wide = wo_ref.shape[0] > channels
+    mine_at = pl.multiple_of(mt * channels, 128) if wide else 0
+    w_pieces = wy_send.shape[0]
+    w_rows = channels // 2 // w_pieces
 
     def peer(s):
         return lax.rem(me + s, ep)
@@ -97,10 +103,11 @@
     ]
     for copy in mix_loads:
         copy.start()
+    wo_place = wo_ref.at[pl.ds(mine_at, channels)]
     weights = [
         pltpu.make_async_copy(src, dst, w_sem.at[i])
         for i, (src, dst) in enumerate(
-            [(wg_hbm, wg_ref), (wu_hbm, wu_ref), (wd_hbm, wd_ref), (wo_hbm, wo_ref)]
+            [(wo_hbm, wo_place), (wg_hbm, wg_ref), (wu_hbm, wu_ref), (wd_hbm, wd_ref)]
         )
     ]
     for copy in weights:
@@ -151,9 +158,53 @@
             q_ref.at[dest], q_all.at[slot], q_send.at[dest], q_recv.at[slot], {"ep": dest}
         )
 
+    def w_part(t, half_of, i):
+        at = pl.multiple_of(t * channels + half_of * (channels // 2) + i * w_rows, 16)
+        return wo_ref.at[pl.ds(at, w_rows)]
+
+    def w_half(t, half_of):
+        at = pl.multiple_of(t * channels + half_of * (channels // 2), 16)
+        return wo_ref.at[pl.ds(at, channels // 2)]
+
+    parity = lax.rem(me, 2)
+
+    def wy_copy(i):
+        at = w_part(mt, parity, i)
+        return remote(at, at, wy_send.at[i], wy_recv.at[i], {"tp": other(1)})
+
+    def wx_copy(i):
+        at = w_part(other(1), parity, i)
+        return remote(at, at, wx_send.at[i], wx_recv.at[i], {"ep": twin})
+
+    def wd_copy(i):
+        at = w_half(mt if i < 2 else other(1), i if i < 2 else (parity if i == 2 else 1 - parity))
+        return remote(at, at, wd_send.at[i], wd_recv.at[i], {"tp": partner})
+
+    def w_across():
+        for i in range(w_pieces):
+            wy_copy(i).wait_recv()
+            wx_copy(i).start()
+        wd_copy(2).start()
+
+    def w_along():
+        for i in range(w_pieces):
+            wx_copy(i).wait_recv()
+        wd_copy(3).start()
+
     tail = pl.ds(ep * cap, tail_rows)
     step = 2 if share % 2 == 0 else 1
     twin = me + 1 - 2 * lax.rem(me, 2)
+
+    def w_start(first, last):
+        for i in range(first, last):
+            wy_copy(i).start()
+
+    weights[0].wait()
+    pl.semaphore_wait(barrier, ep - 1 + 1 + chips - 1)
+    if wide:
+        w_start(0, w_pieces)
+        for i in range(2):
+            wd_copy(i).start()
 
     expert_ids = lax.broadcasted_iota(jnp.int32, (ep, token_count), 0)
     chosen = jnp.zeros((ep, token_count), jnp.float32)
@@ -180,13 +231,16 @@
             jnp.bfloat16
         )
 
-    for s in range(1, ep):
-        x_out[s] = routed(s)
-    pl.semaphore_wait(barrier, ep - 1 + 1 + chips - 1)
-    for s in range(1, ep):
-        x_copy(s).start()
     exp_gain = gains_ref[:, 2 * full :]
     seg_ref[tail, columns(mt)] = jnp.broadcast_to(exp_gain, (tail_rows, width)).astype(jnp.bfloat16)
+    ahead = 3 if ep == 8 else ep
+
+    def send_x(first, last):
+        for s in range(first, last):
+            x_out[s] = routed(s)
+            x_copy(s).start()
+
+    send_x(1, ahead)
     seg_ref[rows(0), columns(mt)] = routed(0)
 
     def rows_of(n):
@@ -270,7 +324,7 @@
                 y_copy(k, s).start()
         d_copy(0, g).wait_recv()
 
-    early = ep // 2 - 1
+    early = ep - 1
 
     def fin(s):
         total = sum_ref[rows(s), columns(mt)].astype(jnp.float32)
@@ -285,10 +339,7 @@
         if 0 < s <= early:
             z_copy(s).start()
 
-    spread(ep)
-    spread(0)
-
-    def send_mix():
+    def make_mix():
         for copy in mix_loads:
             copy.wait()
         gain = gains_ref[:, :full]
@@ -307,8 +358,7 @@
             kv_ref[h] = both[:, h * 128 : (h + 1) * 128].astype(jnp.bfloat16)
         kv_all[me] = kv_ref[me // share]
         for i in range(step, ep, step):
-            dest = lax.rem(me + i, ep)
-            kv_copy(dest, me).start()
+            kv_copy(lax.rem(me + i, ep), me).start()
         if step == 2:
             k_copy(me).start()
         q = project(normed_ref[...], wq_ref[...]) * (1.0 / math.sqrt(head_size))
@@ -328,50 +378,103 @@
                     q_ref[h * share + r] = one[:, h * 128 : (h + 1) * 128].astype(jnp.bfloat16)
         q_all[me] = q_ref[me]
 
-        def send_q(s, _):
-            q_copy(peer(s), me).start()
-            return 0
-
-        lax.fori_loop(1, ep, send_q, 0)
-
     def pass_on(i):
         slot = lax.rem(me - i + ep, ep)
         kv_copy(peer(1), slot).wait_recv()
         k_copy(slot).start()
 
     lane = lax.broadcasted_iota(jnp.int32, (1, 128), 1)
-    send_mix()
-    for n in range(1, ep):
-        spread(n)
-        if n == 1:
-            forward(ep)
-            forward(0)
-        if n >= 3:
-            forward(n - 2)
-    if ep == 1:
-        forward(ep)
-        forward(0)
-    for n in range(max(1, ep - 2), ep):
-        forward(n)
-    for g in range(groups):
-        first, last = g * per, (g + 1) * per
+    spread(ep)
+    spread(0)
+    make_mix()
+
+    def send_q(s, _):
+        q_copy(peer(s), me).start()
+        return 0
+
+    lax.fori_loop(1, ep, send_q, 0)
+
+    def kv_forward():
+        if step == 2:
+            for i in range(2, ep, 2):
+                pass_on(i)
+
+    def collect(g):
         if g == 0:
             gathered(ep)
-            for copy in weights:
+            for copy in weights[1:]:
                 copy.wait()
-        else:
-            pair(g - 1)
-        for s in range(first, last):
+        for s in range(g * per, (g + 1) * per):
             gathered(s)
-        expert(g)
-    if step == 2:
-        for i in range(2, ep, 2):
-            pass_on(i)
 
     def q_wait(s, _):
         q_copy(peer(s), before(s)).wait_recv()
         return 0
 
+    def run_expert(g):
+        collect(g)
+        expert(g)
+
+    def first_forward():
+        forward(ep)
+        forward(0)
+
+    def fins(g):
+        for s in range(g * per, (g + 1) * per):
+            fin(s)
+
+    tasks = []
+
+    def add(when, act, *args):
+        tasks.append((when, functools.partial(act, *args)))
+
+    if ep == 8:
+        add(-1, spread, 1)
+        add(-1, spread, 2)
+        add(-1, kv_forward)
+        add(-1, send_x, ahead, ep)
+        if wide:
+            add(-1, w_across)
+        add(0, first_forward)
+        add(1, spread, 3)
+        add(1, forward, 1)
+        add(2, forward, 2)
+        add(2, spread, 4)
+        add(3, forward, 3)
+        add(4, spread, 5)
+        add(5, forward, 4)
+        add(6, spread, 6)
+        add(7, spread, 7)
+        add(7, forward, 5)
+        add(8, run_expert, 0)
+        add(8, forward, 6)
+        add(8, forward, 7)
+        add(8, pair, 0)
+        add(8, run_expert, 1)
+        add(9, pair, 1)
+        add(9, fins, 0)
+        if wide:
+            add(9, w_along)
+    else:
+        add(-1, kv_forward)
+        for n in range(1, ep):
+            add(ep, spread, n)
+        add(ep, first_forward)
+        for n in range(1, ep):
+            add(ep, forward, n)
+        for g in range(groups):
+            add(ep, run_expert, g)
+            if g > 0:
+                add(ep, pair, g - 1)
+        if wide:
+            add(ep, w_across)
+            add(ep, w_along)
+        for g in range(groups - 1):
+            add(ep, fins, g)
+
+    for when, act in tasks:
+        if when < 0:
+            act()
     lax.fori_loop(1, ep, q_wait, 0)
 
     def queries(i):
@@ -387,7 +490,6 @@
     row = lax.broadcasted_iota(jnp.int32, (part, block), 0) + lax.rem(me, share) * part
     visible = lax.broadcasted_iota(jnp.int32, (part, block), 1) < row
     carry = acc = q_rest = None
-    done = 0
     for n in range(ep):
         j = ep - 1 - n
 
@@ -408,11 +510,9 @@
             carry = jnp.concatenate([new_carry, carry], axis=0)
             acc = jnp.concatenate([new_acc, acc], axis=0)
             q_rest = jnp.concatenate([q, q_rest], axis=0)
-        if n == min(1, ep - 1):
-            pair(groups - 1)
-        if n >= 1:
-            fin(done)
-            done = done + 1
+        for when, act in tasks:
+            if when == n:
+                act()
     for i in range(ep):
         block_out = acc[i * part : (i + 1) * part]
         if packed:
@@ -433,16 +533,16 @@
 
     lax.fori_loop(1, ep, start_a, 0)
     att_all[me] = att_ref[me]
-    for s in range(done, ep):
-        fin(s)
-    for s in range(early + 1, ep):
-        z_copy(s).start()
+    for when, act in tasks:
+        if when == ep:
+            act()
 
     def wait_a(s, _):
         a_copy(peer(s), before(s)).wait_recv()
         return 0
 
     lax.fori_loop(1, ep, wait_a, 0)
+    late = groups - 1
     for r in range(share):
         got = [att_all[h * share + r].astype(jnp.float32) for h in range(heads)]
         if packed:
@@ -464,28 +564,6 @@
     def half_rows(c):
         return pl.ds(pl.multiple_of(c * half, half), half)
 
-    h_copy = remote(m_send, m_got, h_send.at[0], h_recv.at[0], {"tp": partner})
-    m_send[...] = jnp.dot(
-        att_rows[half_rows(1 - core), :], wo_ref[...], preferred_element_type=jnp.float32
-    ).astype(jnp.bfloat16)
-    h_copy.start()
-    mine = jnp.dot(att_rows[half_rows(core), :], wo_ref[...], preferred_element_type=jnp.float32)
-    h_copy.wait_recv()
-
-    def v_copy(k, i):
-        at = pl.ds(i * piece, piece)
-        return remote(
-            m_sum.at[0, at], m_sum.at[k, at], v_send.at[k, i], v_recv.at[k, i],
-            {"tp": other(k)},
-        )
-
-    for i in range(pieces):
-        at = pl.ds(i * piece, piece)
-        pair = mine[i * piece : (i + 1) * piece] + m_got[at, :].astype(jnp.float32)
-        m_sum[0, at, :] = pair.astype(jnp.bfloat16)
-        for k in range(1, chips):
-            v_copy(k, i).start()
-
     def o_copy(i):
         at = out_ref.at[pl.ds(pl.multiple_of(core * half + i * piece, piece), piece)]
         return remote(at, at, o_send.at[i], o_recv.at[i], {"tp": partner})
@@ -508,21 +586,93 @@
                 )
         exp_out_ref[...] = total.astype(jnp.bfloat16)
 
-    for i in range(pieces):
+    def b_copy(j):
+        dest = lax.rem(mt + j, tp)
+        return remote(
+            att_rows.at[half_rows(lax.rem(dest, 2))],
+            att_wide.at[:, pl.ds(mine_at, channels)],
+            b_send.at[j], b_recv.at[j], {"tp": dest},
+        )
+
+    def h_copy():
+        return remote(m_send, m_got, h_send.at[0], h_recv.at[0], {"tp": partner})
+
+    def v_copy(k, i):
         at = pl.ds(i * piece, piece)
-        if i == min(2, pieces - 1):
-            combine()
-        for k in range(1, chips):
-            v_copy(k, i).wait_recv()
-        total = jnp.zeros((piece, out_ref.shape[1]), jnp.float32)
-        for chip in range(chips):
-            slot = lax.rem(mt // 2 - chip + chips, chips)
-            total = total + m_sum[slot, at, :].astype(jnp.float32)
+        return remote(
+            m_sum.at[0, at], m_sum.at[k, at], v_send.at[k, i], v_recv.at[k, i],
+            {"tp": other(k)},
+        )
+
+    def publish(i, total):
         own_rows = pl.ds(pl.multiple_of(core * half + i * piece, piece), piece)
         out_ref[own_rows, :] = normalize(total, gain).astype(jnp.bfloat16)
         o_copy(i).start()
 
-    h_copy.wait_send()
+    if wide:
+        for j in range(1, tp):
+            b_copy(j).start()
+        att_wide[:, pl.ds(mine_at, channels)] = att_rows[half_rows(core), :]
+        for when, act in tasks:
+            if when == ep + 1:
+                act()
+        for i in range(4):
+            wd_copy(i).wait_recv()
+        for j in range(1, tp):
+            b_copy(j).wait_recv()
+        for i in range(pieces):
+            total = jnp.dot(
+                att_wide[i * piece : (i + 1) * piece, :], wo_ref[...],
+                preferred_element_type=jnp.float32,
+            )
+            publish(i, total)
+        fins(late)
+        for s in range(early + 1, ep):
+            z_copy(s).start()
+        combine()
+    else:
+        pair(late)
+        fins(late)
+        for s in range(early + 1, ep):
+            z_copy(s).start()
+        m_send[...] = jnp.dot(
+            att_rows[half_rows(1 - core), :], wo_ref[...], preferred_element_type=jnp.float32
+        ).astype(jnp.bfloat16)
+        h_copy().start()
+        mine = jnp.dot(
+            att_rows[half_rows(core), :], wo_ref[...], preferred_element_type=jnp.float32
+        )
+        h_copy().wait_recv()
+        for i in range(pieces):
+            at = pl.ds(i * piece, piece)
+            both = mine[i * piece : (i + 1) * piece] + m_got[at, :].astype(jnp.float32)
+            m_sum[0, at, :] = both.astype(jnp.bfloat16)
+            for k in range(1, chips):
+                v_copy(k, i).start()
+        combine()
+        for i in range(pieces):
+            at = pl.ds(i * piece, piece)
+            for k in range(1, chips):
+                v_copy(k, i).wait_recv()
+            total = jnp.zeros((piece, out_ref.shape[1]), jnp.float32)
+            for chip in range(chips):
+                slot = lax.rem(mt // 2 - chip + chips, chips)
+                total = total + m_sum[slot, at, :].astype(jnp.float32)
+            publish(i, total)
+
+    if wide:
+        for j in range(1, tp):
+            b_copy(j).wait_send()
+        for i in range(w_pieces):
+            wy_copy(i).wait_send()
+            wx_copy(i).wait_send()
+        for i in range(4):
+            wd_copy(i).wait_send()
+    else:
+        h_copy().wait_send()
+        for k in range(1, chips):
+            for i in range(pieces):
+                v_copy(k, i).wait_send()
     for n in range(ep + 1):
         p_copy(n).wait_send()
         for k in range(1, chips):
@@ -534,8 +684,6 @@
     for k in range(1, chips):
         for s in range(ep):
             y_copy(k, s).wait_send()
-        for i in range(pieces):
-            v_copy(k, i).wait_send()
     for s in range(1, ep):
         x_copy(s).wait_send()
         z_copy(s).wait_send()
@@ -571,6 +719,9 @@
     pieces = 4
     groups = 2 if ep % 2 == 0 else 1
     others = max(chips - 1, 1)
+    channels = wo.shape[0]
+    wide = chips == 2 and packed and ep % 2 == 0 and share % 2 == 0
+    w_pieces = 8
     q_rows = part // 2 if packed else part
     q_stride = head_size if packed else 2 * head_size
     dma = pltpu.SemaphoreType.DMA
@@ -586,8 +737,8 @@
     return pl.pallas_call(
         functools.partial(kernel, (ep, tp, share, part, packed, cap)),
         out_shape=(
-            jax.ShapeDtypeStruct((row_count, full), jnp.bfloat16),
-            jax.ShapeDtypeStruct((token_count, width), jnp.bfloat16),
+            pltpu.VMEM((row_count, full), jnp.bfloat16),
+            pltpu.VMEM((token_count, width), jnp.bfloat16),
         ),
         in_specs=[vmem] * 5 + [hbm] * 8,
         out_specs=(vmem, vmem),
@@ -599,15 +750,20 @@
             held(slots, width),
             held(ep, row_count, 128), held(ep, q_rows, 128),
             held(slots + 16, full),
-            held(*wg.shape), held(*wu.shape), held(*wd.shape), held(*wo.shape),
+            held(*wg.shape), held(*wu.shape), held(*wd.shape),
+            held(tp * channels if wide else channels, full),
             held(slots, full), held(chips, slots, width), held(others, slots, width),
             held(others, slots, width), held(slots, width),
             held(ep, q_rows, 128), held(ep, q_rows, 128), held(row_count, wo.shape[0]),
-            held(half, full), held(half, full), held(chips, half, full),
+            held(*((16, 128) if wide else (half, full))),
+            held(*((16, 128) if wide else (half, full))),
+            held(*((1, 16, 128) if wide else (chips, half, full))),
+            held(*((half, tp * channels) if wide else (16, 128))),
         ]
         + both(ep) + [dma((ep,))] + both(ep) + both(ep) + both(ep + 1) + both(chips, ep + 1)
         + both(chips, ep + 1) + both(chips, groups) + both(chips, ep) + both(ep) + both(ep)
-        + both(1) + both(chips, pieces) + both(pieces) + [dma((1 + 3 * heads,)), dma((4,))],
+        + both(1) + both(chips, pieces) + both(pieces) + both(tp) + both(w_pieces)
+        + both(w_pieces) + both(4) + [dma((1 + 3 * heads,)), dma((4,))],
         compiler_params=pltpu.CompilerParams(
             collective_id=0, has_side_effects=True, vmem_limit_bytes=60 * 1024 * 1024
         ),
@@ -642,7 +798,8 @@
     token_count, top_count = routes.shape
     experts = w_gate.shape[0] * ep
     capacity = 4 * token_count * top_count // (3 * experts)
-    gains = jnp.concatenate([mix_gain, out_gain, exp_gain]).astype(jnp.float32)[None]
+    gains = jnp.concatenate([mix_gain, out_gain, exp_gain]).astype(jnp.float32)
+    gains = lax.optimization_barrier(gains)[None]
     if not packed:
         w_out = w_out.reshape(heads_here, head_size, -1)
         w_out = jnp.concatenate([jnp.zeros_like(w_out), w_out], axis=1)

time: 76.8 us -> 71.4 us (0.930)
  local copies, waits for them, and re-layouts: 5.05 us -> 2.23 us
  Pallas kernels: 70.2 us -> 67.6 us
    pallas_call x1, Pallas kernels: 70.2 us -> 67.6 us  [one_call(): pl.pallas_call(functools.partial(kernel, (ep, tp, share, part, packed, ca...]
    concatenate x3 -> x0, local copies, waits for them, and re-layouts: 2.07 us -> none  [on_device(): jnp.concatenate([mix_gain, out_gain, exp_gain]).astype(jnp.float32)[None]]
    unnamed x4 -> x2, local copies, waits for them, and re-layouts: 2.98 us -> 1.61 us
where the time goes in v2:
time: 71.4 us; the launch traced here: 71.1 us
  Pallas kernels  67.6 us (95%)
  local copies, waits for them, and re-layouts  2.23 us (3%)
  other arithmetic  0.72 us (1%)
    pallas_call x1, Pallas kernels, one_call(): pl.pallas_call(functools.partial(kernel, (ep, tp, share, part, packed, ca...  67.6 us
    unnamed x2, local copies, waits for them, and re-layouts  1.61 us

profile of v2, /device:TPU:0, one launch (start us, length us, event | category | flops | bytes accessed | tf_op | source)
XLA Modules:
  0.0 71.1 jit_solution(973412085906423413)
XLA Ops:
  0.6 0.7 %maximum_convert_fusion = f32[4608]{0:T(1024)S(1)} fusion(bf16[512]{0:T(512)(128)(2,1)} %param.24, bf16[2048]{0:T(1024)(128)(2,1)} %param.22, bf16[2048]{0:T(1024)(128)(2,1)} %param.16), kind=kLoop, calls=%fused_computation | loop fusion | flops 27648 | bytes 27648 | tf_op jit(solution)/shard_map/convert_element_type | solution.py:801
  1.4 0.6 broadcast_in_dim.3.gains_ref
  2.0 67.6 %shard_map.158 = (bf16[256,2048]{1,0:T(8,128)(2,1)S(1)}, bf16[96,512]{1,0:T(8,128)(2,1)S(1)}) custom-call(s32[4,96]{1,0:T(4,128)} %bitcast.8, f32[4,96]{1,0:T(4,128)} %bitcast.9, f32[1,4608]{1,0:T(1,128)} %broadcast_in_dim.3.gains_ref, f32[4,2048]{1,0:T(4,128)} %off_ref.1, bf16[96,512]{1,0:T(8,128)(2,1)} %exp_ref.1, bf16[256,2048]{1,0:T(8,128)(2,1)} %mix_hbm.1, ...), custom_call_target="tpu_custom_call" | custom-call | tf_op jit(solution)/shard_map/pallas_call | solution.py:737
  69.5 1.0 %copy.19 = bf16[256,2048]{1,0:T(8,128)(2,1)} copy(bf16[256,2048]{1,0:T(8,128)(2,1)S(1)} %get-tuple-element.2) | data formatting | bytes 2097152
  70.5 0.6 copy.20

commit v3 on v2

--- a/solution.py
+++ b/solution.py
@@ -180,11 +180,12 @@
         at = w_half(mt if i < 2 else other(1), i if i < 2 else (parity if i == 2 else 1 - parity))
         return remote(at, at, wd_send.at[i], wd_recv.at[i], {"tp": partner})
 
-    def w_across():
-        for i in range(w_pieces):
+    def w_across(first, last):
+        for i in range(first, last):
             wy_copy(i).wait_recv()
             wx_copy(i).start()
-        wd_copy(2).start()
+        if last == w_pieces:
+            wd_copy(2).start()
 
     def w_along():
         for i in range(w_pieces):
@@ -199,10 +200,11 @@
         for i in range(first, last):
             wy_copy(i).start()
 
+    w_first = 5 if ep == 8 else w_pieces
     weights[0].wait()
     pl.semaphore_wait(barrier, ep - 1 + 1 + chips - 1)
     if wide:
-        w_start(0, w_pieces)
+        w_start(0, w_first)
         for i in range(2):
             wd_copy(i).start()
 
@@ -233,7 +235,7 @@
 
     exp_gain = gains_ref[:, 2 * full :]
     seg_ref[tail, columns(mt)] = jnp.broadcast_to(exp_gain, (tail_rows, width)).astype(jnp.bfloat16)
-    ahead = 3 if ep == 8 else ep
+    ahead = per if ep == 8 else ep
 
     def send_x(first, last):
         for s in range(first, last):
@@ -313,16 +315,26 @@
         for k in list(range(1, chips)) + [0]:
             d_copy(k, g).start()
 
-    def pair(g):
+    def pair_start(g):
         for k in range(1, chips):
             d_copy(k, g).wait_recv()
-        for s in range(g * per, (g + 1) * per):
+        pair_rows(range(g * per, g * per + per // 2))
+
+    def pair_end(g):
+        pair_rows(range(g * per + per // 2, (g + 1) * per))
+        d_copy(0, g).wait_recv()
+
+    def pair(g):
+        pair_start(g)
+        pair_end(g)
+
+    def pair_rows(these):
+        for s in these:
             for k in range(1, chips):
                 mine = sum_ref[rows(s), columns(other(k))].astype(jnp.float32)
                 both = mine + e_got[k, rows(s), :].astype(jnp.float32)
                 e_pair[k - 1, rows(s), :] = both.astype(jnp.bfloat16)
                 y_copy(k, s).start()
-        d_copy(0, g).wait_recv()
 
     early = ep - 1
 
@@ -431,27 +443,32 @@
     if ep == 8:
         add(-1, spread, 1)
         add(-1, spread, 2)
+        add(-1, spread, 3)
+        if wide:
+            add(-1, w_start, w_first, w_pieces)
         add(-1, kv_forward)
         add(-1, send_x, ahead, ep)
         if wide:
-            add(-1, w_across)
-        add(0, first_forward)
-        add(1, spread, 3)
-        add(1, forward, 1)
-        add(2, forward, 2)
+            add(-1, w_across, 0, w_first)
+        add(-1, first_forward)
+        add(-1, forward, 1)
+        add(0, forward, 2)
+        add(1, forward, 3)
         add(2, spread, 4)
-        add(3, forward, 3)
-        add(4, spread, 5)
+        add(2, run_expert, 0)
+        add(2, spread, 5)
+        if wide:
+            add(4, w_across, w_first, w_pieces)
+        add(3, spread, 6)
+        add(4, spread, 7)
         add(5, forward, 4)
-        add(6, spread, 6)
-        add(7, spread, 7)
+        add(5, pair, 0)
         add(7, forward, 5)
-        add(8, run_expert, 0)
         add(8, forward, 6)
         add(8, forward, 7)
-        add(8, pair, 0)
         add(8, run_expert, 1)
-        add(9, pair, 1)
+        add(8, pair_start, 1)
+        add(9, pair_end, 1)
         add(9, fins, 0)
         if wide:
             add(9, w_along)
@@ -467,7 +484,7 @@
             if g > 0:
                 add(ep, pair, g - 1)
         if wide:
-            add(ep, w_across)
+            add(ep, w_across, 0, w_pieces)
             add(ep, w_along)
         for g in range(groups - 1):
             add(ep, fins, g)
@@ -618,6 +635,7 @@
                 act()
         for i in range(4):
             wd_copy(i).wait_recv()
+        fins(late)
         for j in range(1, tp):
             b_copy(j).wait_recv()
         for i in range(pieces):
@@ -626,7 +644,6 @@
                 preferred_element_type=jnp.float32,
             )
             publish(i, total)
-        fins(late)
         for s in range(early + 1, ep):
             z_copy(s).start()
         combine()

time: 71.4 us -> 64.8 us (0.908)
  Pallas kernels: 67.6 us -> 61 us
    pallas_call x1, Pallas kernels: 67.6 us -> 61 us  [one_call(): pl.pallas_call(functools.partial(kernel, (ep, tp, share, part, packed, ca...]
where the time goes in v3:
time: 64.8 us; the launch traced here: 64.6 us
  Pallas kernels  61 us (94%)
  local copies, waits for them, and re-layouts  2.23 us (3%)
  other arithmetic  0.72 us (1%)
    pallas_call x1, Pallas kernels, one_call(): pl.pallas_call(functools.partial(kernel, (ep, tp, share, part, packed, ca...  61 us
    unnamed x2, local copies, waits for them, and re-layouts  1.61 us

profile of v3, /device:TPU:0, one launch (start us, length us, event | category | flops | bytes accessed | tf_op | source)
XLA Modules:
  0.0 64.6 jit_solution(3666759442338853446)
XLA Ops:
  0.6 0.7 %maximum_convert_fusion = f32[4608]{0:T(1024)S(1)} fusion(bf16[512]{0:T(512)(128)(2,1)} %param.24, bf16[2048]{0:T(1024)(128)(2,1)} %param.22, bf16[2048]{0:T(1024)(128)(2,1)} %param.16), kind=kLoop, calls=%fused_computation | loop fusion | flops 27648 | bytes 27648 | tf_op jit(solution)/shard_map/convert_element_type | solution.py:818
  1.4 0.6 broadcast_in_dim.3.gains_ref
  2.0 61.0 %shard_map.158 = (bf16[256,2048]{1,0:T(8,128)(2,1)S(1)}, bf16[96,512]{1,0:T(8,128)(2,1)S(1)}) custom-call(s32[4,96]{1,0:T(4,128)} %bitcast.8, f32[4,96]{1,0:T(4,128)} %bitcast.9, f32[1,4608]{1,0:T(1,128)} %broadcast_in_dim.3.gains_ref, f32[4,2048]{1,0:T(4,128)} %off_ref.1, bf16[96,512]{1,0:T(8,128)(2,1)} %exp_ref.1, bf16[256,2048]{1,0:T(8,128)(2,1)} %mix_hbm.1, ...), custom_call_target="tpu_custom_call" | custom-call | tf_op jit(solution)/shard_map/pallas_call | solution.py:754
  63.0 1.0 %copy.19 = bf16[256,2048]{1,0:T(8,128)(2,1)} copy(bf16[256,2048]{1,0:T(8,128)(2,1)S(1)} %get-tuple-element.2) | data formatting | bytes 2097152
  63.9 0.6 copy.20

commit v4 on v3

--- a/solution.py
+++ b/solution.py
@@ -53,7 +53,7 @@
     out_ref, exp_out_ref,
     mix_ref, normed_ref, wq_ref, wkv_ref, kv_ref, q_ref, x_out, key_ref, weight_ref, ret_ref,
     kv_all, q_all, seg_ref, wg_ref, wu_ref, wd_ref, wo_ref, sum_ref, e_got, e_pair, e_y, e_fin,
-    att_ref, att_all, att_rows, m_send, m_got, m_sum, att_wide,
+    att_ref, att_all, att_rows, m_send, m_got, m_sum, att_wide, mix_back,
     kv_send, kv_recv, k_send, q_send, q_recv, x_send, x_recv, p_send, p_recv, g_send, g_recv,
     f_send, f_recv, d_send, d_recv, y_send, y_recv, z_send, z_recv, a_send, a_recv,
     h_send, h_recv, v_send, v_recv, o_send, o_recv, b_send, b_recv, wy_send, wy_recv,
@@ -76,6 +76,9 @@
     piece = half // pieces
     groups = d_send.shape[1]
     per = ep // groups
+    spans = [(g * per, (g + 1) * per) for g in range(groups)]
+    if ep == 8:
+        spans = [(0, 4), (4, 6), (6, 8)]
     channels = wo_hbm.shape[0]
     wide = wo_ref.shape[0] > channels
     mine_at = pl.multiple_of(mt * channels, 128) if wide else 0
@@ -233,9 +236,9 @@
             jnp.bfloat16
         )
 
-    exp_gain = gains_ref[:, 2 * full :]
+    exp_gain = gains_ref[2 * full :][None]
     seg_ref[tail, columns(mt)] = jnp.broadcast_to(exp_gain, (tail_rows, width)).astype(jnp.bfloat16)
-    ahead = per if ep == 8 else ep
+    ahead = 4 if ep == 8 else ep
 
     def send_x(first, last):
         for s in range(first, last):
@@ -277,8 +280,11 @@
         for k in range(1, chips):
             f_copy(n, k).wait_recv()
 
+    def group_rows(g):
+        return pl.ds(spans[g][0] * cap, (spans[g][1] - spans[g][0]) * cap)
+
     def d_copy(k, g):
-        at = pl.ds(g * per * cap, per * cap)
+        at = group_rows(g)
         return remote(
             sum_ref.at[at, columns(lax.rem(partner + 2 * k, tp))], e_got.at[k, at],
             d_send.at[k, g], d_recv.at[k, g], {"tp": partner},
@@ -303,7 +309,7 @@
         )
 
     def expert(g):
-        at = pl.ds(g * per * cap, per * cap)
+        at = group_rows(g)
         gains = seg_ref[tail, :][:1]
         segment = normalize(seg_ref[at, :].astype(jnp.float32), gains).astype(jnp.bfloat16)
         gate_pre = jnp.dot(segment, wg_ref[...], preferred_element_type=jnp.float32)
@@ -318,10 +324,9 @@
     def pair_start(g):
         for k in range(1, chips):
             d_copy(k, g).wait_recv()
-        pair_rows(range(g * per, g * per + per // 2))
+        pair_rows(range(*spans[g]))
 
     def pair_end(g):
-        pair_rows(range(g * per + per // 2, (g + 1) * per))
         d_copy(0, g).wait_recv()
 
     def pair(g):
@@ -354,7 +359,7 @@
     def make_mix():
         for copy in mix_loads:
             copy.wait()
-        gain = gains_ref[:, :full]
+        gain = gains_ref[:full][None]
         chunk = min(64, block)
         for r in range(0, block, chunk):
             at = pl.ds(r, chunk)
@@ -416,7 +421,7 @@
             gathered(ep)
             for copy in weights[1:]:
                 copy.wait()
-        for s in range(g * per, (g + 1) * per):
+        for s in range(*spans[g]):
             gathered(s)
 
     def q_wait(s, _):
@@ -432,8 +437,16 @@
         forward(0)
 
     def fins(g):
-        for s in range(g * per, (g + 1) * per):
+        for s in range(*spans[g]):
             fin(s)
+
+    def weigh():
+        for s in range(ep):
+            e = peer(s)
+            spread_to = jnp.where(placed(e), weight_ref[pl.ds(e, 1), :], 0.0)
+            high = spread_to.astype(jnp.bfloat16).astype(jnp.float32)
+            both = jnp.concatenate([high, spread_to - high], axis=0)
+            mix_back[s] = both.T.astype(jnp.bfloat16)
 
     tasks = []
 
@@ -461,15 +474,20 @@
             add(4, w_across, w_first, w_pieces)
         add(3, spread, 6)
         add(4, spread, 7)
-        add(5, forward, 4)
+        add(4, forward, 4)
         add(5, pair, 0)
-        add(7, forward, 5)
-        add(8, forward, 6)
+        add(5, forward, 5)
+        add(7, forward, 6)
+        add(8, run_expert, 1)
         add(8, forward, 7)
-        add(8, run_expert, 1)
+        add(8, weigh)
         add(8, pair_start, 1)
+        add(8, run_expert, 2)
+        add(8, fins, 0)
+        add(8, pair_start, 2)
         add(9, pair_end, 1)
-        add(9, fins, 0)
+        add(9, pair_end, 2)
+        add(9, fins, 1)
         if wide:
             add(9, w_along)
     else:
@@ -488,6 +506,7 @@
             add(ep, w_along)
         for g in range(groups - 1):
             add(ep, fins, g)
+        add(ep, weigh)
 
     for when, act in tasks:
         if when < 0:
@@ -585,22 +604,18 @@
         at = out_ref.at[pl.ds(pl.multiple_of(core * half + i * piece, piece), piece)]
         return remote(at, at, o_send.at[i], o_recv.at[i], {"tp": partner})
 
-    gain = gains_ref[:, full : 2 * full]
+    gain = gains_ref[full : 2 * full][None]
 
     def combine():
         total = jnp.zeros((token_count, width), jnp.float32)
         for s in range(ep):
             if s > 0:
                 z_arrived(s).wait_recv()
-            e = peer(s)
-            spread_to = jnp.where(placed(e), weight_ref[pl.ds(e, 1), :], 0.0)
-            high = spread_to.astype(jnp.bfloat16).astype(jnp.float32)
-            both = jnp.concatenate([high, spread_to - high], axis=0).T.astype(jnp.bfloat16)
-            got = ret_ref[pl.ds(pl.multiple_of(e * cap, cap), cap), :]
-            for low in range(2):
-                total = total + jnp.dot(
-                    both[:, low * cap : (low + 1) * cap], got, preferred_element_type=jnp.float32
-                )
+            got = ret_ref[pl.ds(pl.multiple_of(peer(s) * cap, cap), cap), :]
+            total = total + jnp.dot(
+                mix_back[s], jnp.concatenate([got, got], axis=0),
+                preferred_element_type=jnp.float32,
+            )
         exp_out_ref[...] = total.astype(jnp.bfloat16)
 
     def b_copy(j):
@@ -625,6 +640,46 @@
         own_rows = pl.ds(pl.multiple_of(core * half + i * piece, piece), piece)
         out_ref[own_rows, :] = normalize(total, gain).astype(jnp.bfloat16)
         o_copy(i).start()
+
+    def drain():
+        if wide:
+            for j in range(1, tp):
+                b_copy(j).wait_send()
+            for i in range(w_pieces):
+                wy_copy(i).wait_send()
+                wx_copy(i).wait_send()
+            for i in range(4):
+                wd_copy(i).wait_send()
+        else:
+            h_copy().wait_send()
+            for k in range(1, chips):
+                for i in range(pieces):
+                    v_copy(k, i).wait_send()
+        for n in range(ep + 1):
+            p_copy(n).wait_send()
+            for k in range(1, chips):
+                g_copy(n, k).wait_send()
+                f_copy(n, k).wait_send()
+        for k in range(chips):
+            for g in range(groups):
+                d_copy(k, g).wait_send()
+        for k in range(1, chips):
+            for s in range(ep):
+                y_copy(k, s).wait_send()
+        for s in range(1, ep):
+            x_copy(s).wait_send()
+
+        def finish(s, _):
+            q_copy(peer(s), me).wait_send()
+            a_copy(peer(s), me).wait_send()
+            return 0
+
+        lax.fori_loop(1, ep, finish, 0)
+        for i in range(step, ep, step):
+            kv_copy(lax.rem(me + i, ep), me).wait_send()
+        if step == 2:
+            for i in range(0, ep, 2):
+                k_copy(lax.rem(me - i + ep, ep)).wait_send()
 
     if wide:
         for j in range(1, tp):
@@ -644,8 +699,7 @@
                 preferred_element_type=jnp.float32,
             )
             publish(i, total)
-        for s in range(early + 1, ep):
-            z_copy(s).start()
+        drain()
         combine()
     else:
         pair(late)
@@ -676,46 +730,10 @@
                 slot = lax.rem(mt // 2 - chip + chips, chips)
                 total = total + m_sum[slot, at, :].astype(jnp.float32)
             publish(i, total)
-
-    if wide:
-        for j in range(1, tp):
-            b_copy(j).wait_send()
-        for i in range(w_pieces):
-            wy_copy(i).wait_send()
-            wx_copy(i).wait_send()
-        for i in range(4):
-            wd_copy(i).wait_send()
-    else:
-        h_copy().wait_send()
-        for k in range(1, chips):
-            for i in range(pieces):
-                v_copy(k, i).wait_send()
-    for n in range(ep + 1):
-        p_copy(n).wait_send()
-        for k in range(1, chips):
-            g_copy(n, k).wait_send()
-            f_copy(n, k).wait_send()
-    for k in range(chips):
-        for g in range(groups):
-            d_copy(k, g).wait_send()
-    for k in range(1, chips):
-        for s in range(ep):
-            y_copy(k, s).wait_send()
+        drain()
+
     for s in range(1, ep):
-        x_copy(s).wait_send()
         z_copy(s).wait_send()
-
-    def finish(s, _):
-        q_copy(peer(s), me).wait_send()
-        a_copy(peer(s), me).wait_send()
-        return 0
-
-    lax.fori_loop(1, ep, finish, 0)
-    for i in range(step, ep, step):
-        kv_copy(lax.rem(me + i, ep), me).wait_send()
-    if step == 2:
-        for i in range(0, ep, 2):
-            k_copy(lax.rem(me - i + ep, ep)).wait_send()
     for i in range(pieces):
         at = out_ref.at[pl.ds(pl.multiple_of((1 - core) * half + i * piece, piece), piece)]
         remote(at, at, o_send.at[i], o_recv.at[i], {"tp": partner}).wait_recv()
@@ -734,10 +752,11 @@
     chips = tp // 2
     half = row_count // 2
     pieces = 4
-    groups = 2 if ep % 2 == 0 else 1
+    groups = 3 if ep == 8 else 2 if ep % 2 == 0 else 1
     others = max(chips - 1, 1)
     channels = wo.shape[0]
     wide = chips == 2 and packed and ep % 2 == 0 and share % 2 == 0
+    pieces = 2 if wide else 4
     w_pieces = 8
     q_rows = part // 2 if packed else part
     q_stride = head_size if packed else 2 * head_size
@@ -776,6 +795,7 @@
             held(*((16, 128) if wide else (half, full))),
             held(*((1, 16, 128) if wide else (chips, half, full))),
             held(*((half, tp * channels) if wide else (16, 128))),
+            held(ep, token_count, 2 * cap),
         ]
         + both(ep) + [dma((ep,))] + both(ep) + both(ep) + both(ep + 1) + both(chips, ep + 1)
         + both(chips, ep + 1) + both(chips, groups) + both(chips, ep) + both(ep) + both(ep)
@@ -816,7 +836,6 @@
     experts = w_gate.shape[0] * ep
     capacity = 4 * token_count * top_count // (3 * experts)
     gains = jnp.concatenate([mix_gain, out_gain, exp_gain]).astype(jnp.float32)
-    gains = lax.optimization_barrier(gains)[None]
     if not packed:
         w_out = w_out.reshape(heads_here, head_size, -1)
         w_out = jnp.concatenate([jnp.zeros_like(w_out), w_out], axis=1)

time: 64.8 us -> 63.5 us (0.980)
  Pallas kernels: 61 us -> 59.7 us
    pallas_call x1, Pallas kernels: 61 us -> 59.7 us  [one_call(): pl.pallas_call(functools.partial(kernel, (ep, tp, share, part, packed, ca...]
where the time goes in v4:
time: 63.5 us; the launch traced here: 63.3 us
  Pallas kernels  59.7 us (94%)
  local copies, waits for them, and re-layouts  1.61 us (3%)
  other arithmetic  1.33 us (2%)
  between operations  0.64 us (1%)
    pallas_call x1, Pallas kernels, one_call(): pl.pallas_call(functools.partial(kernel, (ep, tp, share, part, packed, ca...  59.7 us
    unnamed x2, local copies, waits for them, and re-layouts  1.61 us
    convert_element_type x1, other arithmetic, on_device(): gains = jnp.concatenate([mix_gain, out_gain, exp_gain]).astype(jnp.float32)  1.33 us

profile of v4, /device:TPU:0, one launch (start us, length us, event | category | flops | bytes accessed | tf_op | source)
XLA Modules:
  0.0 63.3 jit_solution(10249917534106031549)
XLA Ops:
  0.6 1.3 %maximum_convert_fusion.gains_ref = f32[4608]{0:T(1024)} fusion(bf16[512]{0:T(512)(128)(2,1)} %param.24, bf16[2048]{0:T(1024)(128)(2,1)} %param.22, bf16[2048]{0:T(1024)(128)(2,1)} %param.16), kind=kLoop, calls=%fused_computation | loop fusion | flops 27648 | bytes 27648 | tf_op jit(solution)/shard_map/convert_element_type | solution.py:838
  2.0 59.7 %shard_map.158 = (bf16[256,2048]{1,0:T(8,128)(2,1)S(1)}, bf16[96,512]{1,0:T(8,128)(2,1)S(1)}) custom-call(s32[4,96]{1,0:T(4,128)} %bitcast.8, f32[4,96]{1,0:T(4,128)} %bitcast.9, f32[4608]{0:T(1024)} %maximum_convert_fusion.gains_ref, f32[4,2048]{1,0:T(4,128)} %off_ref.1, bf16[96,512]{1,0:T(8,128)(2,1)} %exp_ref.1, bf16[256,2048]{1,0:T(8,128)(2,1)} %mix_hbm.1, ...), custom_call_target="tpu_custom_call" | custom-call | tf_op jit(solution)/shard_map/pallas_call | solution.py:773
  61.7 1.0 %copy.19 = bf16[256,2048]{1,0:T(8,128)(2,1)} copy(bf16[256,2048]{1,0:T(8,128)(2,1)S(1)} %get-tuple-element.2) | data formatting | bytes 2097152
  62.6 0.6 %copy.20 = bf16[96,512]{1,0:T(8,128)(2,1)} copy(bf16[96,512]{1,0:T(8,128)(2,1)S(1)} %get-tuple-element.3) | data formatting | bytes 196608
